TPU v7x, 32 devices: a whole 2x2x4 slice. The times are simulated.
32 devices in a mesh: ep: 8 (over z, y), tp: 4 (over x, core).
Axes of the slice: x: 2, y: 2, z: 4, core: 2. Of those that a mesh axis runs over, the one named last changes fastest.
Arguments:
- mixer_in: bfloat16 [3072, 2048], P(('ep', 'tp')), may hold values from -6 to 6
- expert_in: bfloat16 [3072, 2048], P(('ep', 'tp')), may hold values from -6 to 6
- mixer_gain: float32 [2048], replicated, may hold values from 0.1 to 1.9
- in_gate_weight: bfloat16 [2048, 2048], P(None, 'tp'), may hold values from -0.125 to 0.125
- out_gate_weight: bfloat16 [2048, 2048], P(None, 'tp'), may hold values from -0.125 to 0.125
- value_weight: bfloat16 [2048, 2048], P(None, 'tp'), may hold values from -0.125 to 0.125
- conv_taps: float32 [3, 2048], replicated, may hold values from -3 to 3
- mixer_proj: bfloat16 [2048, 2048], P(None, 'tp'), may hold values from -0.125 to 0.125
- expert_gain: float32 [2048], replicated, may hold values from 0.1 to 1.9
- route_ids: int32 [3072, 2], P('ep'), may hold values from 0 to 7, all different within a row; in each aligned block of 96 rows (0 to 95, 96 to 191, ...) at most 48 rows name the same one
- route_weights: float32 [3072, 2], P('ep'), may hold values from 0.1 to 1
- gate_weight: bfloat16 [8, 2048, 1024], P('ep', None, 'tp'), may hold values from -0.125 to 0.125
- up_weight: bfloat16 [8, 2048, 1024], P('ep', None, 'tp'), may hold values from -0.125 to 0.125
- down_weight: bfloat16 [8, 1024, 2048], P('ep', None, 'tp'), may hold values from -0.1875 to 0.1875
Outputs:
- mixer_out: bfloat16 [3072, 2048], P('ep', 'tp')
- expert_out: bfloat16 [3072, 2048], P('ep', 'tp')
Inputs may be any that keep to these rules, and one draw needn't show every extreme that they name: `route_ids`: each row names 2 different experts. In each aligned block of 96 rows no expert is named by more than 48 rows, a bound that some block reaches.
All inputs are finite; a program needn't handle non-finite values.
Results may differ from a plain program's by a relative error of at most 0.0076.
Values may be sent and summed in bfloat16 or wider, within the bound.
A program may use at most 64 MiB of HBM per device.

v0:
```python
import functools

import jax
import jax.numpy as jnp
from jax import lax
from jax.experimental import pallas as pl
from jax.experimental.pallas import tpu as pltpu
from jax.sharding import PartitionSpec as P

norm_eps = 1e-06


def passed_along(value, axis, steps):
    count = lax.axis_size(axis)
    leading, last = (max(0, -steps), min(count, count - steps))
    return lax.ppermute(value, axis, [(source, source + steps) for source in range(leading, last)])


def rms_rows(values, gain_row):
    wide = values.astype(jnp.float32)
    scale = lax.rsqrt(jnp.mean(wide * wide, axis=-1, keepdims=True) + norm_eps)
    return (wide * scale * gain_row).astype(jnp.bfloat16)


def place_slots(route_ids, group_rows, experts, slot_cap):
    row_total, top_count = route_ids.shape
    groups = row_total // group_rows
    labels = jnp.arange(experts, dtype=jnp.int32)
    onehot = (
        route_ids.reshape(groups, group_rows * top_count)[:, :, None] == labels[None, None, :]
    ).astype(jnp.int32)
    earlier = jnp.cumsum(onehot, axis=1) - onehot
    within = jnp.sum(earlier * onehot, axis=2)
    slot_index = jnp.arange(groups, dtype=jnp.int32)[:, None] * slot_cap + within
    return slot_index.reshape(row_total, top_count)


def on_device(
    mixer_in,
    expert_in,
    mixer_gain,
    in_gate_weight,
    out_gate_weight,
    value_weight,
    conv_taps,
    mixer_proj,
    expert_gain,
    route_ids,
    route_weights,
    gate_weight,
    up_weight,
    down_weight,
):
    tok_dev = mixer_in.shape[0]
    tp_count = lax.axis_size("tp")
    ep_count = lax.axis_size("ep")
    top_count = route_ids.shape[1]
    experts = ep_count * gate_weight.shape[0]
    slot_cap = max(2, 2 * tok_dev * top_count // experts)
    tp_index = lax.axis_index("tp")
    mixer_normed = rms_rows(mixer_in, mixer_gain)
    expert_normed = rms_rows(expert_in, expert_gain)
    block_slot = place_slots(route_ids, tok_dev, experts, slot_cap)
    mixer_rows = lax.all_gather(mixer_normed, "tp", axis=0, tiled=True)
    send_ids = lax.dynamic_slice_in_dim(route_ids, tp_index * tok_dev, tok_dev, 0)
    send_slot = (
        lax.dynamic_slice_in_dim(block_slot, tp_index * tok_dev, tok_dev, 0) - tp_index * slot_cap
    )
    source_count = expert_normed.shape[0]
    flat_index = (send_ids * slot_cap + send_slot).reshape(-1)
    row_table = (
        jnp.full((experts * slot_cap,), source_count, jnp.int32)
        .at[flat_index]
        .set(jnp.repeat(jnp.arange(source_count, dtype=jnp.int32), top_count))
    )
    padded_rows = jnp.concatenate(
        [expert_normed, jnp.zeros((1, expert_normed.shape[1]), jnp.bfloat16)], axis=0
    )
    outgoing = padded_rows[row_table].reshape(experts, slot_cap, expert_normed.shape[1])
    arrived = lax.all_to_all(outgoing, "ep", split_axis=0, concat_axis=0, tiled=True)
    arrived = lax.all_gather(arrived, "tp", axis=1, tiled=True)
    chan_width = in_gate_weight.shape[1]
    in_gate = jnp.dot(mixer_rows, in_gate_weight, preferred_element_type=jnp.float32)
    out_gate = jnp.dot(mixer_rows, out_gate_weight, preferred_element_type=jnp.float32)
    values = jnp.dot(mixer_rows, value_weight, preferred_element_type=jnp.float32)
    product = (in_gate * values).astype(jnp.bfloat16)
    tap_count = conv_taps.shape[0]
    rim_rows = passed_along(product[product.shape[0] - (tap_count - 1) :], "ep", 1)
    extended = jnp.concatenate([rim_rows, product], axis=0).astype(jnp.float32)
    tap_rows = lax.dynamic_slice_in_dim(conv_taps, tp_index * chan_width, chan_width, 1)
    row_count = product.shape[0]
    conv_sum = tap_rows[0] * extended[0:row_count]
    for tap_index in range(1, tap_count):
        conv_sum = conv_sum + tap_rows[tap_index] * extended[tap_index : tap_index + row_count]
    gated = (out_gate * conv_sum).astype(jnp.bfloat16)
    slots_in = arrived.reshape(-1, arrived.shape[2])
    gate_pre = jnp.dot(slots_in, gate_weight[0], preferred_element_type=jnp.float32)
    up_pre = jnp.dot(slots_in, up_weight[0], preferred_element_type=jnp.float32)
    hidden = (jax.nn.silu(gate_pre) * up_pre).astype(jnp.bfloat16)
    down_slice = down_weight[0]
    gated_all, hidden_all = (
        lax.all_gather(gated, "tp", axis=1, tiled=True),
        lax.all_gather(hidden, "tp", axis=1, tiled=True),
    )
    mixer_sum = jnp.dot(gated_all, mixer_proj, preferred_element_type=jnp.float32)
    expert_sum = jnp.dot(hidden_all, down_slice, preferred_element_type=jnp.float32)
    mixer_out = mixer_sum.astype(jnp.bfloat16)
    results = expert_sum.astype(jnp.bfloat16).reshape(ep_count, -1, expert_sum.shape[1])
    returned = lax.all_to_all(results, "ep", split_axis=0, concat_axis=0, tiled=True)
    back_index = (route_ids * (tp_count * slot_cap) + block_slot).reshape(-1)
    picked = returned.reshape(-1, returned.shape[2])[back_index].reshape(
        route_ids.shape[0], top_count, -1
    )
    shares = route_weights / jnp.sum(route_weights, axis=1, keepdims=True)
    expert_out = jnp.sum(picked.astype(jnp.float32) * shares[:, :, None], axis=1).astype(
        jnp.bfloat16
    )
    return (mixer_out, expert_out)


MESH = pl.DeviceIdType.MESH
F32 = jnp.float32
BF16 = jnp.bfloat16
VMEM_BYTES = 60 * 1024 * 1024


def dot(a, b):
    return jnp.dot(a, b, preferred_element_type=F32)


def prepare_kernel(
    slot_cap, mixer_in, expert_in, mixer_gain, expert_gain, ids, weights,
    normed, own_rows, outgoing, partner_table, combine,
):
    tok_dev = mixer_in.shape[0]
    blocks = ids.shape[0] // tok_dev
    slots = combine.shape[1]
    experts = slots // slot_cap
    me = lax.axis_index("tp")
    normed[...] = rms_rows(mixer_in[...], mixer_gain[...])
    rows = rms_rows(expert_in[...], expert_gain[...])
    own_rows[...] = rows
    partner = (me + 2) % blocks
    below = (
        lax.broadcasted_iota(jnp.int32, (tok_dev, tok_dev), 1)
        < lax.broadcasted_iota(jnp.int32, (tok_dev, tok_dev), 0)
    ).astype(BF16)
    labels = lax.broadcasted_iota(jnp.int32, (tok_dev, 128), 1)
    places = lax.broadcasted_iota(jnp.int32, (tok_dev, slots), 1)
    chosen = jnp.zeros((tok_dev, slots), F32)
    theirs = jnp.zeros((tok_dev, slots), F32)
    for block in range(blocks):
        part = pl.ds(block * tok_dev, tok_dev)
        picks = ids.shape[1]
        named = [ids[part, k : k + 1] for k in range(picks)]
        share = [weights[part, k : k + 1] for k in range(picks)]
        total = functools.reduce(jnp.add, share)
        hot = [(labels == n).astype(F32) for n in named]
        rank = dot(below, functools.reduce(jnp.add, hot).astype(BF16))
        mixed = jnp.zeros((tok_dev, slots), F32)
        sent = jnp.zeros((tok_dev, slots), F32)
        for k in range(picks):
            within = jnp.sum(rank * hot[k], axis=1, keepdims=True).astype(jnp.int32)
            spot = places == named[k] * slot_cap + within
            mixed = mixed + jnp.where(spot, share[k] / total, 0.0)
            sent = sent + jnp.where(spot, 1.0, 0.0)
        combine[part, :] = mixed
        chosen = jnp.where(me == block, sent, chosen)
        theirs = jnp.where(partner == block, sent, theirs)
    table = jnp.transpose(chosen).astype(BF16)
    partner_table[...] = jnp.transpose(theirs).astype(BF16).reshape(experts, slot_cap, tok_dev)
    for expert in range(experts):
        outgoing[expert] = dot(table[expert * slot_cap : (expert + 1) * slot_cap], rows).astype(BF16)


MIX_AT = (0, 3, 4, 5, 8, 9)

LAGS = (0, 1, 2, 4, 5)

DISP, F2, F1, G1, H2, H1, HG, RET, DISP2 = range(9)
M2, M1, MG, Q2, Q1, QG, RIM, DX = range(8)


def chunk_order(count):
    half = count // 2
    far, close = list(range(half, count)), list(range(half))
    return close[:1] + far + close[1:]


def exchange_kernel(
    normed, own_rows, outgoing, partner_table, combine, taps,
    w_in, w_out, w_val, w_proj, w_gate, w_up, w_down,
    mixer_out, expert_out,
    v_in, v_out, v_val, v_proj, v_gate, v_up, v_down,
    rows, arrived, hid, res, returned, gates, ext, rim_out, rim_in, gated, dense, outgoing2,
    send, recv, send1, recv1, wsem,
):
    count = outgoing.shape[0]
    group, tok_dev, width = rows.shape
    half = count // 2
    chan = v_in.shape[1]
    slot_cap = outgoing.shape[1]
    hid_width = v_gate.shape[1]
    e = lax.axis_index("ep")
    t = lax.axis_index("tp")
    t1 = t + 1 - 2 * (t % 2)
    t2 = (t + 2) % group
    t3 = (t1 + 2) % group

    loads = [
        pltpu.make_async_copy(a, b, wsem.at[n])
        for n, (a, b) in enumerate(
            [(w_in, v_in), (w_val, v_val), (w_out, v_out), (w_gate.at[0], v_gate),
             (w_up.at[0], v_up), (w_down.at[0], v_down), (w_proj, v_proj)]
        )
    ]
    for load in loads:
        load.start()

    def mixed_with(s):
        value, bit = 0, 1
        while bit < count:
            value = value + ((e // bit + s // bit) % 2) * bit
            bit *= 2
        return value

    order = chunk_order(count)

    def shift_of(i):
        return functools.reduce(jnp.add, [jnp.where(i == n, s, 0) for n, s in enumerate(order)])

    def source_of(i):
        return mixed_with(shift_of(i))

    barrier = pltpu.get_barrier_semaphore()
    for s in range(1, count):
        pl.semaphore_signal(barrier, inc=1, device_id=(mixed_with(s), t), device_id_type=MESH)
    for peer in (t1, t2):
        pl.semaphore_signal(barrier, inc=1, device_id=(e, peer), device_id_type=MESH)
    pl.semaphore_wait(barrier, count + 1)

    def chunk(kind, i, src, dst, dev):
        return pltpu.make_async_remote_copy(
            src_ref=src, dst_ref=dst, send_sem=send.at[kind, i], recv_sem=recv.at[kind, i],
            device_id=dev, device_id_type=MESH,
        )

    def once(kind, src, dst, dev):
        return pltpu.make_async_remote_copy(
            src_ref=src, dst_ref=dst, send_sem=send1.at[kind], recv_sem=recv1.at[kind],
            device_id=dev, device_id_type=MESH,
        )

    near, across = (e, t1), (e, t2)
    after = ((e + 1) % count, t)

    def disp(i):
        return chunk(DISP, i, outgoing.at[source_of(i)], arrived.at[e, t], (source_of(i), t))

    def ret(i):
        return chunk(RET, i, res.at[source_of(i)], returned.at[e], (source_of(i), t))

    def came(kind, i, dst):
        chunk(kind, i, dst, dst, near).wait_recv()

    def came_once(kind, dst):
        once(kind, dst, dst, near).wait_recv()

    def disp2(i):
        src = source_of(i)
        return chunk(DISP2, i, outgoing2.at[shift_of(i)], arrived.at[e, t2], (src, t))

    once(DX, own_rows, dense, across).start()

    def start_disp(i, carry):
        @pl.when(shift_of(i) != 0)
        def _():
            disp(i).start()

        return carry

    lax.fori_loop(0, count, start_disp, 0)
    rows[t] = normed[...]
    arrived[e, t] = outgoing[e]
    once(M1, normed, rows.at[t], near).start()
    came_once(DX, dense)

    def pass_on(i, carry):
        shift = shift_of(i)

        @pl.when(shift < half)
        def _():
            picked = dot(partner_table[source_of(i)], dense[...]).astype(BF16)

            @pl.when(shift == 0)
            def _():
                arrived[e, t2] = picked

            @pl.when(shift != 0)
            def _():
                outgoing2[shift] = picked
                disp2(i).start()

        return carry

    lax.fori_loop(0, count, pass_on, 0)

    def finish(i):
        src = source_of(i)
        came(H1, i, hid.at[src, t1])
        came(HG, i, hid.at[src, t3])
        total = dot(hid[src, 0], v_down[0:hid_width, :])
        for other in range(1, group):
            total += dot(hid[src, other], v_down[other * hid_width : (other + 1) * hid_width, :])
        total = total.astype(BF16).reshape(group, slot_cap, chan)

        @pl.when(shift_of(i) != 0)
        def _():
            res[src] = total
            ret(i).start()

        @pl.when(shift_of(i) == 0)
        def _():
            returned[src] = total

    def hand_hidden(i):
        src = source_of(i)
        came(H2, i, hid.at[src, t2])
        chunk(HG, i, hid.at[src, t2], hid.at[src, t2], near).start()

    def expand(i):
        src = source_of(i)
        came(F1, i, arrived.at[src, t1])
        came(G1, i, arrived.at[src, t3])
        x = arrived[src].reshape(group * slot_cap, width)
        gate = dot(x, v_gate[...])
        up = dot(x, v_up[...])
        hid[src, t] = (gate / (1.0 + jnp.exp(-gate)) * up).astype(BF16)
        chunk(H2, i, hid.at[src, t], hid.at[src, t], across).start()
        chunk(H1, i, hid.at[src, t], hid.at[src, t], near).start()

    def hand_rows(i):
        src = source_of(i)
        shift = shift_of(i)

        @pl.when(shift >= half)
        def _():
            came(F2, i, arrived.at[src, t2])

        @pl.when((shift < half) & (shift != 0))
        def _():
            came(DISP2, i, arrived.at[src, t2])

        chunk(G1, i, arrived.at[src, t2], arrived.at[src, t2], near).start()

    def take(i):
        src = source_of(i)

        @pl.when(shift_of(i) != 0)
        def _():
            came(DISP, i, arrived.at[src, t])

        @pl.when(shift_of(i) >= half)
        def _():
            chunk(F2, i, arrived.at[src, t], arrived.at[src, t], across).start()

        chunk(F1, i, arrived.at[src, t], arrived.at[src, t], near).start()

    all_rows = group * tok_dev
    tile = 256

    def mixer_products():
        came_once(M1, rows.at[t1])
        came_once(MG, rows.at[t3])

        def one(n, carry):
            cols = pl.ds(pl.multiple_of(n * tile, tile), tile)
            x = rows[...].reshape(all_rows, width)
            product = (dot(x, v_in[:, cols]) * dot(x, v_val[:, cols])).astype(BF16)
            ext[pl.ds(8, all_rows), cols] = product.astype(F32)
            rim_out[:, cols] = product[all_rows - 16 :]
            gates[:, cols] = dot(x, v_out[:, cols])
            return carry

        lax.fori_loop(0, chan // tile, one, 0)
        once(RIM, rim_out, rim_in, after).start()

    def mixer_conv():
        came_once(RIM, rim_in)
        edge = rim_in[...].astype(F32)[8:16]
        ext[0:8, :] = jnp.where(e == 0, jnp.zeros_like(edge), edge)
        tap_count = taps.shape[0]
        total = taps[0:1, :] * ext[pl.ds(8 - (tap_count - 1), all_rows), :]
        for n in range(1, tap_count):
            total += taps[n : n + 1, :] * ext[pl.ds(8 - (tap_count - 1) + n, all_rows), :]
        gated[t] = (gates[...] * total).astype(BF16)
        once(Q2, gated.at[t], gated.at[t], across).start()
        once(Q1, gated.at[t], gated.at[t], near).start()

    def mixer_project():
        came_once(Q1, gated.at[t1])
        came_once(QG, gated.at[t3])

        def one(n, carry):
            cols = pl.ds(pl.multiple_of(n * tile, tile), tile)
            total = dot(gated[0], v_proj[0:chan, cols])
            for other in range(1, group):
                total += dot(gated[other], v_proj[other * chan : (other + 1) * chan, cols])
            mixer_out[:, cols] = total.astype(BF16)
            return carry

        lax.fori_loop(0, chan // tile, one, 0)

    stages = (take, hand_rows, expand, hand_hidden, finish)

    def step(i, carry):
        for stage, lag in reversed(list(zip(stages, LAGS))):
            @pl.when((i >= lag) & (i < count + lag))
            def _(stage=stage, lag=lag):
                stage(i - lag)

        @pl.when(i == MIX_AT[0])
        def _():
            once(M2, normed, rows.at[t], across).start()
            for load in loads:
                load.wait()

        @pl.when(i == MIX_AT[1])
        def _():
            came_once(M2, rows.at[t2])
            once(MG, rows.at[t2], rows.at[t2], near).start()

        @pl.when(i == MIX_AT[2])
        def _():
            mixer_products()

        @pl.when(i == MIX_AT[3])
        def _():
            mixer_conv()

        @pl.when(i == MIX_AT[4])
        def _():
            came_once(Q2, gated.at[t2])
            once(QG, gated.at[t2], gated.at[t2], near).start()

        @pl.when(i == MIX_AT[5])
        def _():
            mixer_project()

        return carry

    lax.fori_loop(0, count + LAGS[-1], step, 0)

    def landed(i, carry):
        @pl.when(shift_of(i) != 0)
        def _():
            came(RET, i, returned.at[source_of(i)])

        return carry

    lax.fori_loop(0, count, landed, 0)
    for block in range(group):
        part = pl.ds(block * tok_dev, tok_dev)
        mix = combine[part, :]
        high = mix.astype(BF16)
        low = (mix - high.astype(F32)).astype(BF16)
        values = returned[:, block].reshape(count * slot_cap, chan)
        expert_out[part, :] = (dot(high, values) + dot(low, values)).astype(BF16)

    def drain(i, carry):
        src = source_of(i)
        chunk(F1, i, arrived.at[src, t], arrived.at[src, t], near).wait_send()

        @pl.when(shift_of(i) >= half)
        def _():
            chunk(F2, i, arrived.at[src, t], arrived.at[src, t], near).wait_send()

        @pl.when(shift_of(i) != 0)
        def _():
            disp(i).wait_send()
            ret(i).wait_send()

        @pl.when((shift_of(i) != 0) & (shift_of(i) < half))
        def _():
            disp2(i).wait_send()

        chunk(G1, i, arrived.at[src, t2], arrived.at[src, t2], near).wait_send()
        for kind in (H2, H1):
            chunk(kind, i, hid.at[src, t], hid.at[src, t], near).wait_send()
        chunk(HG, i, hid.at[src, t2], hid.at[src, t2], near).wait_send()
        return carry

    lax.fori_loop(0, count, drain, 0)
    for kind in (M2, M1):
        once(kind, normed, rows.at[t], near).wait_send()
    once(MG, rows.at[t2], rows.at[t2], near).wait_send()
    once(DX, own_rows, dense, near).wait_send()
    for kind in (Q2, Q1):
        once(kind, gated.at[t], gated.at[t], near).wait_send()
    once(QG, gated.at[t2], gated.at[t2], near).wait_send()
    once(RIM, rim_out, rim_in, after).wait_send()


def write_kernel(mixer_sum, expert_sum, mixer_out, expert_out, sem):
    copies = [
        pltpu.make_async_copy(a, b, sem.at[n])
        for n, (a, b) in enumerate([(mixer_sum, mixer_out), (expert_sum, expert_out)])
    ]
    for copy in copies:
        copy.start()
    for copy in copies:
        copy.wait()


def fused_on_device(
    mixer_in, expert_in, mixer_gain, in_gate_weight, out_gate_weight, value_weight, conv_taps,
    mixer_proj, expert_gain, route_ids, route_weights, gate_weight, up_weight, down_weight,
):
    tok_dev, width = mixer_in.shape
    group = lax.axis_size("tp")
    count = lax.axis_size("ep")
    experts = count * gate_weight.shape[0]
    slot_cap = 2 * tok_dev * route_ids.shape[1] // experts
    chan = in_gate_weight.shape[1]
    hid_width = gate_weight.shape[2]
    all_rows = group * tok_dev
    vm = pl.BlockSpec(memory_space=pltpu.VMEM)
    anywhere = pl.BlockSpec(memory_space=pl.ANY)
    shape = jax.ShapeDtypeStruct
    normed, own_rows, outgoing, partner_table, combine = pl.pallas_call(
        functools.partial(prepare_kernel, slot_cap),
        out_shape=(
            shape((tok_dev, width), BF16),
            shape((tok_dev, width), BF16),
            shape((experts, slot_cap, width), BF16),
            shape((experts, slot_cap, tok_dev), BF16),
            shape((all_rows, experts * slot_cap), F32),
        ),
        in_specs=[vm] * 6,
        out_specs=(vm,) * 5,
        compiler_params=pltpu.CompilerParams(vmem_limit_bytes=VMEM_BYTES // 2),
        name="prepare",
    )(mixer_in, expert_in, mixer_gain[None, :], expert_gain[None, :], route_ids, route_weights)
    taps = lax.dynamic_slice_in_dim(conv_taps, lax.axis_index("tp") * chan, chan, 1)
    weights = (
        in_gate_weight, out_gate_weight, value_weight, mixer_proj, gate_weight, up_weight, down_weight,
    )
    dma = pltpu.SemaphoreType.DMA
    results = pl.pallas_call(
        exchange_kernel,
        out_shape=(shape((all_rows, chan), BF16), shape((all_rows, chan), BF16)),
        in_specs=[vm] * 6 + [pl.BlockSpec(memory_space=pltpu.HBM)] * 7,
        out_specs=(vm, vm),
        scratch_shapes=[
            pltpu.VMEM(w.shape[-2:], BF16)
            for w in (in_gate_weight, out_gate_weight, value_weight, mixer_proj,
                      gate_weight, up_weight, down_weight)
        ] + [
            pltpu.VMEM((group, tok_dev, width), BF16),
            pltpu.VMEM((count, group, slot_cap, width), BF16),
            pltpu.VMEM((count, group, group * slot_cap, hid_width), BF16),
            pltpu.VMEM((count, group, slot_cap, chan), BF16),
            pltpu.VMEM((count, group, slot_cap, chan), BF16),
            pltpu.VMEM((all_rows, chan), F32),
            pltpu.VMEM((all_rows + 8, chan), F32),
            pltpu.VMEM((16, chan), BF16),
            pltpu.VMEM((16, chan), BF16),
            pltpu.VMEM((group, all_rows, chan), BF16),
            pltpu.VMEM((tok_dev, width), BF16),
            pltpu.VMEM((count // 2, slot_cap, width), BF16),
            dma((9, count)), dma((9, count)), dma((8,)), dma((8,)), dma((7,)),
        ],
        compiler_params=pltpu.CompilerParams(
            collective_id=0, has_side_effects=True, vmem_limit_bytes=VMEM_BYTES * 3 // 4
        ),
        name="exchange",
    )(normed, own_rows, outgoing, partner_table, combine, taps, *weights)
    return pl.pallas_call(
        write_kernel,
        out_shape=(shape((all_rows, chan), BF16), shape((all_rows, chan), BF16)),
        in_specs=[vm, vm],
        out_specs=(anywhere, anywhere),
        scratch_shapes=[dma((2,))],
        name="write",
    )(*results)


def body_for(mesh):
    count, group = mesh.shape["ep"], mesh.shape["tp"]

    def body(*args):
        tok_dev, picks, held = args[0].shape[0], args[9].shape[1], args[11].shape[0]
        slot_cap = 2 * tok_dev * picks // (count * held)
        fits = count in (4, 8, 16) and group == 4 and held == 1 and slot_cap % 16 == 0
        return (fused_on_device if fits and tok_dev % 16 == 0 else on_device)(*args)

    return body


def solution(mesh):
    return jax.shard_map(
        body_for(mesh),
        mesh=mesh,
        in_specs=(
            P(("ep", "tp"), None),
            P(("ep", "tp"), None),
            P(),
            P(None, "tp"),
            P(None, "tp"),
            P(None, "tp"),
            P(),
            P(None, "tp"),
            P(),
            P("ep", None),
            P("ep", None),
            P("ep", None, "tp"),
            P("ep", None, "tp"),
            P("ep", None, "tp"),
        ),
        out_specs=(P("ep", "tp"), P("ep", "tp")),
        check_vma=False,
    )
```

profile of v0, /device:TPU:0, one launch (start us, length us, event | category | flops | bytes accessed | tf_op | source)
XLA Modules:
  0.0 104.4 jit_solution(18059490754492527236)
XLA Ops:
  0.6 0.0 copy-start
  0.6 0.0 copy-start.2
  0.7 0.7 copy-done
  1.4 0.8 copy.16.ids
  2.2 0.8 copy.17.weights
  3.0 0.0 copy-start.7
  3.1 1.0 copy-done.7
  4.0 0.0 copy-start.8
  4.0 1.0 copy-done.8
  5.0 0.0 copy-start.9
  5.0 0.7 copy-done.9
  5.7 0.0 copy-start.10
  5.7 0.7 copy-done.10
  6.4 1.8 %prepare.1 = (bf16[96,2048]{1,0:T(8,128)(2,1)S(1)}, bf16[96,2048]{1,0:T(8,128)(2,1)S(1)}, bf16[8,48,2048]{2,1,0:T(8,128)(2,1)S(1)}, bf16[8,48,96]{2,1,0:T(8,128)(2,1)S(1)}, f32[384,384]{1,0:T(8,128)S(1)}) custom-call(bf16[96,2048]{1,0:T(8,128)(2,1)S(1)} %copy-done.7, bf16[96,2048]{1,0:T(8,128)(2,1)S(1)} %copy-done.8, f32[1,2048]{1,0:T(1,128)S(1)} %bitcast.2, ...), custom_call_target="tpu_custom_call" | custom-call | tf_op jit(solution)/shard_map/prepare/pallas_call | solution.py:530
  8.3 0.0 copy-done.2
  8.3 0.0 copy-start.1
  8.3 1.6 %copy-done.1 = bf16[2048,512]{1,0:T(8,128)(2,1)S(1)} copy-done((bf16[2048,512]{1,0:T(8,128)(2,1)S(1)}, bf16[2048,512]{1,0:T(8,128)(2,1)}, u32[]{:S(2)}) %copy-start.1) | copy-done | bytes 2097176
  9.9 0.0 copy-start.3
  9.9 1.2 %copy-done.3 = bf16[1,2048,256]{2,1,0:T(8,128)(2,1)S(1)} copy-done((bf16[1,2048,256]{2,1,0:T(8,128)(2,1)S(1)}, bf16[1,2048,256]{2,1,0:T(8,128)(2,1)}, u32[]{:S(2)}) %copy-start.3) | copy-done | bytes 1048600
  11.1 0.0 copy-start.4
  11.1 1.2 %copy-done.4 = bf16[1,1024,512]{2,1,0:T(8,128)(2,1)S(1)} copy-done((bf16[1,1024,512]{2,1,0:T(8,128)(2,1)S(1)}, bf16[1,1024,512]{2,1,0:T(8,128)(2,1)}, u32[]{:S(2)}) %copy-start.4) | copy-done | bytes 1048600
  12.3 88.6 %exchange.1 = (bf16[384,512]{1,0:T(8,128)(2,1)S(1)}, bf16[384,512]{1,0:T(8,128)(2,1)S(1)}) custom-call(bf16[96,2048]{1,0:T(8,128)(2,1)S(1)} %get-tuple-element.9.normed, bf16[96,2048]{1,0:T(8,128)(2,1)S(1)} %get-tuple-element.10.own_rows, bf16[8,48,2048]{2,1,0:T(8,128)(2,1)S(1)} %get-tuple-element.11.outgoing, ...), custom_call_target="tpu_custom_call" | custom-call | tf_op jit(solution)/shard_map/exchange/pallas_call | solution.py:549
  100.9 0.0 copy-start.5
  100.9 0.7 copy-done.5
  101.7 0.0 copy-start.6
  101.7 0.7 copy-done.6
  102.4 2.0 %write.1 = (bf16[384,512]{1,0:T(8,128)(2,1)}, bf16[384,512]{1,0:T(8,128)(2,1)}) custom-call(bf16[384,512]{1,0:T(8,128)(2,1)} %copy-done.5, bf16[384,512]{1,0:T(8,128)(2,1)} %copy-done.6), custom_call_target="tpu_custom_call" | custom-call | tf_op jit(solution)/shard_map/write/pallas_call | solution.py:578
  (1 shorter events, 0.0 us)
Async XLA Ops:
  0.6 0.8 copy-start
  0.6 7.6 %copy-start.2 = (bf16[1,2048,256]{2,1,0:T(8,128)(2,1)S(1)}, bf16[1,2048,256]{2,1,0:T(8,128)(2,1)}, u32[]{:S(2)}) copy-start(bf16[1,2048,256]{2,1,0:T(8,128)(2,1)} %w_gate.1) | copy-start | bytes 3145732
  3.0 1.0 copy-start.7
  4.0 1.0 copy-start.8
  5.0 0.7 copy-start.9
  5.7 0.7 copy-start.10
  8.3 1.6 %copy-start.1 = (bf16[2048,512]{1,0:T(8,128)(2,1)S(1)}, bf16[2048,512]{1,0:T(8,128)(2,1)}, u32[]{:S(2)}) copy-start(bf16[2048,512]{1,0:T(8,128)(2,1)} %w_in.1) | copy-start | bytes 6291460
  9.9 1.2 %copy-start.3 = (bf16[1,2048,256]{2,1,0:T(8,128)(2,1)S(1)}, bf16[1,2048,256]{2,1,0:T(8,128)(2,1)}, u32[]{:S(2)}) copy-start(bf16[1,2048,256]{2,1,0:T(8,128)(2,1)} %w_up.1) | copy-start | bytes 3145732
  11.1 1.2 %copy-start.4 = (bf16[1,1024,512]{2,1,0:T(8,128)(2,1)S(1)}, bf16[1,1024,512]{2,1,0:T(8,128)(2,1)}, u32[]{:S(2)}) copy-start(bf16[1,1024,512]{2,1,0:T(8,128)(2,1)} %w_down.1) | copy-start | bytes 3145732
  100.9 0.7 copy-start.5
  101.7 0.7 copy-start.6
where the time goes:
time: 105 us; the launch traced here: 104 us
  Pallas kernels  92.4 us (88%)
  local copies, waits for them, and re-layouts  11.3 us (11%)
    pallas_call x1, Pallas kernels, fused_on_device(): pl.pallas_call(exchange_kernel, out_shape=(shape((all_rows, chan), BF16),...  88.6 us
    unnamed x24, local copies, waits for them, and re-layouts  11.3 us

commit v1 on v0

--- a/solution.py
+++ b/solution.py
@@ -128,19 +128,16 @@
     return jnp.dot(a, b, preferred_element_type=F32)
 
 
-def prepare_kernel(
-    slot_cap, mixer_in, expert_in, mixer_gain, expert_gain, ids, weights,
-    normed, own_rows, outgoing, partner_table, combine,
-):
-    tok_dev = mixer_in.shape[0]
-    blocks = ids.shape[0] // tok_dev
+def prepare(slot_cap, me, expert_in, expert_gain, ids, weights, own_rows, outgoing, partner_table, combine):
+    tok_dev = expert_in.shape[0]
+    picks, all_rows = ids.shape
+    blocks = all_rows // tok_dev
     slots = combine.shape[1]
     experts = slots // slot_cap
-    me = lax.axis_index("tp")
-    normed[...] = rms_rows(mixer_in[...], mixer_gain[...])
-    rows = rms_rows(expert_in[...], expert_gain[...])
-    own_rows[...] = rows
+    rows = own_rows[...]
     partner = (me + 2) % blocks
+    filler = jnp.zeros((8 - 2 * picks, all_rows), F32)
+    columns = jnp.transpose(jnp.concatenate([ids[...].astype(F32), weights[...], filler], axis=0))
     below = (
         lax.broadcasted_iota(jnp.int32, (tok_dev, tok_dev), 1)
         < lax.broadcasted_iota(jnp.int32, (tok_dev, tok_dev), 0)
@@ -150,10 +147,9 @@
     chosen = jnp.zeros((tok_dev, slots), F32)
     theirs = jnp.zeros((tok_dev, slots), F32)
     for block in range(blocks):
-        part = pl.ds(block * tok_dev, tok_dev)
-        picks = ids.shape[1]
-        named = [ids[part, k : k + 1] for k in range(picks)]
-        share = [weights[part, k : k + 1] for k in range(picks)]
+        part = slice(block * tok_dev, (block + 1) * tok_dev)
+        named = [columns[part, k : k + 1].astype(jnp.int32) for k in range(picks)]
+        share = [columns[part, picks + k : picks + k + 1] for k in range(picks)]
         total = functools.reduce(jnp.add, share)
         hot = [(labels == n).astype(F32) for n in named]
         rank = dot(below, functools.reduce(jnp.add, hot).astype(BF16))
@@ -188,12 +184,14 @@
 
 
 def exchange_kernel(
-    normed, own_rows, outgoing, partner_table, combine, taps,
+    mixer_in, expert_in, mixer_gain, expert_gain, ids, shares, all_taps,
     w_in, w_out, w_val, w_proj, w_gate, w_up, w_down,
     mixer_out, expert_out,
     v_in, v_out, v_val, v_proj, v_gate, v_up, v_down,
+    v_mixer, v_expert, v_mixer_gain, v_expert_gain, v_ids, v_shares, taps,
+    normed, own_rows, outgoing, partner_table, combine,
     rows, arrived, hid, res, returned, gates, ext, rim_out, rim_in, gated, dense, outgoing2,
-    send, recv, send1, recv1, wsem,
+    send, recv, send1, recv1, wsem, fsem,
 ):
     count = outgoing.shape[0]
     group, tok_dev, width = rows.shape
@@ -207,6 +205,16 @@
     t2 = (t + 2) % group
     t3 = (t1 + 2) % group
 
+    firsts = [
+        pltpu.make_async_copy(a, b, fsem.at[n])
+        for n, (a, b) in enumerate(
+            [(expert_in, v_expert), (expert_gain, v_expert_gain), (ids, v_ids), (shares, v_shares),
+             (mixer_in, v_mixer), (mixer_gain, v_mixer_gain),
+             (all_taps.at[:, pl.ds(pl.multiple_of(t * chan, 128), chan)], taps)]
+        )
+    ]
+    for load in firsts:
+        load.start()
     loads = [
         pltpu.make_async_copy(a, b, wsem.at[n])
         for n, (a, b) in enumerate(
@@ -214,9 +222,6 @@
              (w_up.at[0], v_up), (w_down.at[0], v_down), (w_proj, v_proj)]
         )
     ]
-    for load in loads:
-        load.start()
-
     def mixed_with(s):
         value, bit = 0, 1
         while bit < count:
@@ -237,6 +242,11 @@
         pl.semaphore_signal(barrier, inc=1, device_id=(mixed_with(s), t), device_id_type=MESH)
     for peer in (t1, t2):
         pl.semaphore_signal(barrier, inc=1, device_id=(e, peer), device_id_type=MESH)
+    for load in firsts[:4]:
+        load.wait()
+    for load in loads:
+        load.start()
+    own_rows[...] = rms_rows(v_expert[...], v_expert_gain[...])
     pl.semaphore_wait(barrier, count + 1)
 
     def chunk(kind, i, src, dst, dev):
@@ -271,6 +281,9 @@
         return chunk(DISP2, i, outgoing2.at[shift_of(i)], arrived.at[e, t2], (src, t))
 
     once(DX, own_rows, dense, across).start()
+    prepare(
+        slot_cap, t, v_expert, v_expert_gain, v_ids, v_shares, own_rows, outgoing, partner_table, combine
+    )
 
     def start_disp(i, carry):
         @pl.when(shift_of(i) != 0)
@@ -280,6 +293,9 @@
         return carry
 
     lax.fori_loop(0, count, start_disp, 0)
+    for load in firsts[4:]:
+        load.wait()
+    normed[...] = rms_rows(v_mixer[...], v_mixer_gain[...])
     rows[t] = normed[...]
     arrived[e, t] = outgoing[e]
     once(M1, normed, rows.at[t], near).start()
@@ -501,14 +517,16 @@
     once(RIM, rim_out, rim_in, after).wait_send()
 
 
-def write_kernel(mixer_sum, expert_sum, mixer_out, expert_out, sem):
-    copies = [
-        pltpu.make_async_copy(a, b, sem.at[n])
-        for n, (a, b) in enumerate([(mixer_sum, mixer_out), (expert_sum, expert_out)])
-    ]
-    for copy in copies:
+def write_kernel(mixer_sum, expert_sum, mixer_out, expert_out, held, sem):
+    pairs = [(mixer_sum, mixer_out), (expert_sum, expert_out)]
+    inward = [pltpu.make_async_copy(a, held.at[n], sem.at[n]) for n, (a, _) in enumerate(pairs)]
+    outward = [pltpu.make_async_copy(held.at[n], b, sem.at[2 + n]) for n, (_, b) in enumerate(pairs)]
+    for copy in inward:
         copy.start()
-    for copy in copies:
+    for first, second in zip(inward, outward):
+        first.wait()
+        second.start()
+    for copy in outward:
         copy.wait()
 
 
@@ -527,21 +545,6 @@
     vm = pl.BlockSpec(memory_space=pltpu.VMEM)
     anywhere = pl.BlockSpec(memory_space=pl.ANY)
     shape = jax.ShapeDtypeStruct
-    normed, own_rows, outgoing, partner_table, combine = pl.pallas_call(
-        functools.partial(prepare_kernel, slot_cap),
-        out_shape=(
-            shape((tok_dev, width), BF16),
-            shape((tok_dev, width), BF16),
-            shape((experts, slot_cap, width), BF16),
-            shape((experts, slot_cap, tok_dev), BF16),
-            shape((all_rows, experts * slot_cap), F32),
-        ),
-        in_specs=[vm] * 6,
-        out_specs=(vm,) * 5,
-        compiler_params=pltpu.CompilerParams(vmem_limit_bytes=VMEM_BYTES // 2),
-        name="prepare",
-    )(mixer_in, expert_in, mixer_gain[None, :], expert_gain[None, :], route_ids, route_weights)
-    taps = lax.dynamic_slice_in_dim(conv_taps, lax.axis_index("tp") * chan, chan, 1)
     weights = (
         in_gate_weight, out_gate_weight, value_weight, mixer_proj, gate_weight, up_weight, down_weight,
     )
@@ -549,13 +552,25 @@
     results = pl.pallas_call(
         exchange_kernel,
         out_shape=(shape((all_rows, chan), BF16), shape((all_rows, chan), BF16)),
-        in_specs=[vm] * 6 + [pl.BlockSpec(memory_space=pltpu.HBM)] * 7,
+        in_specs=[pl.BlockSpec(memory_space=pltpu.HBM)] * 14,
         out_specs=(vm, vm),
         scratch_shapes=[
             pltpu.VMEM(w.shape[-2:], BF16)
             for w in (in_gate_weight, out_gate_weight, value_weight, mixer_proj,
                       gate_weight, up_weight, down_weight)
         ] + [
+            pltpu.VMEM((tok_dev, width), BF16),
+            pltpu.VMEM((tok_dev, width), BF16),
+            pltpu.VMEM((1, width), F32),
+            pltpu.VMEM((1, width), F32),
+            pltpu.VMEM(route_ids.shape[::-1], jnp.int32),
+            pltpu.VMEM(route_ids.shape[::-1], F32),
+            pltpu.VMEM((conv_taps.shape[0], chan), F32),
+            pltpu.VMEM((tok_dev, width), BF16),
+            pltpu.VMEM((tok_dev, width), BF16),
+            pltpu.VMEM((experts, slot_cap, width), BF16),
+            pltpu.VMEM((experts, slot_cap, tok_dev), BF16),
+            pltpu.VMEM((all_rows, experts * slot_cap), F32),
             pltpu.VMEM((group, tok_dev, width), BF16),
             pltpu.VMEM((count, group, slot_cap, width), BF16),
             pltpu.VMEM((count, group, group * slot_cap, hid_width), BF16),
@@ -568,19 +583,23 @@
             pltpu.VMEM((group, all_rows, chan), BF16),
             pltpu.VMEM((tok_dev, width), BF16),
             pltpu.VMEM((count // 2, slot_cap, width), BF16),
-            dma((9, count)), dma((9, count)), dma((8,)), dma((8,)), dma((7,)),
+            dma((9, count)), dma((9, count)), dma((8,)), dma((8,)), dma((7,)), dma((7,)),
         ],
         compiler_params=pltpu.CompilerParams(
-            collective_id=0, has_side_effects=True, vmem_limit_bytes=VMEM_BYTES * 3 // 4
+            collective_id=0, has_side_effects=True, vmem_limit_bytes=VMEM_BYTES
         ),
         name="exchange",
-    )(normed, own_rows, outgoing, partner_table, combine, taps, *weights)
+    )(
+        mixer_in, expert_in, mixer_gain[None, :], expert_gain[None, :],
+        route_ids.T, route_weights.T, conv_taps, *weights,
+    )
     return pl.pallas_call(
         write_kernel,
         out_shape=(shape((all_rows, chan), BF16), shape((all_rows, chan), BF16)),
-        in_specs=[vm, vm],
+        in_specs=[anywhere, anywhere],
         out_specs=(anywhere, anywhere),
-        scratch_shapes=[dma((2,))],
+        scratch_shapes=[pltpu.VMEM((2, all_rows, chan), BF16), dma((4,))],
+        compiler_params=pltpu.CompilerParams(vmem_limit_bytes=VMEM_BYTES),
         name="write",
     )(*results)
 

time: 105 us -> 94 us (0.90)
  local copies, waits for them, and re-layouts: 11.3 us -> 0 us
    unnamed x24 -> x0, local copies, waits for them, and re-layouts: 11.3 us -> none
    pallas_call x1, Pallas kernels: 88.6 us -> 91 us  [fused_on_device(): pl.pallas_call(exchange_kernel, out_shape=(shape((all_rows, chan), BF16),...]
    pallas_call x1 -> x0, Pallas kernels: 1.83 us -> none  [fused_on_device(): pl.pallas_call(functools.partial(prepare_kernel, slot_cap), out_shape=(sh...]
where the time goes in v1:
time: 94 us; the launch traced here: 93.5 us
  Pallas kernels  92.9 us (99%)
    pallas_call x1, Pallas kernels, fused_on_device(): pl.pallas_call(exchange_kernel, out_shape=(shape((all_rows, chan), BF16),...  91 us
    pallas_call x1, Pallas kernels, fused_on_device(): pl.pallas_call(write_kernel, out_shape=(shape((all_rows, chan), BF16), sh...  1.91 us

profile of v1, /device:TPU:0, one launch (start us, length us, event | category | flops | bytes accessed | tf_op | source)
XLA Modules:
  0.0 93.5 jit_solution(18268700609613509979)
XLA Ops:
  0.6 91.0 %exchange.1 = (bf16[384,512]{1,0:T(8,128)(2,1)}, bf16[384,512]{1,0:T(8,128)(2,1)}) custom-call(bf16[96,2048]{1,0:T(8,128)(2,1)} %mixer_in.1, bf16[96,2048]{1,0:T(8,128)(2,1)} %expert_in.1, f32[1,2048]{1,0:T(1,128)} %bitcast.4, f32[1,2048]{1,0:T(1,128)} %bitcast.5, s32[2,384]{1,0:T(2,128)} %bitcast.6, f32[2,384]{1,0:T(2,128)} %bitcast.7, f32[3,2048]{1,0:T(4,128)} %all_taps.1, ...), custom_call_target="tpu_custom_call" | custom-call | tf_op jit(solution)/shard_map/exchange/pallas_call | solution.py:552
  91.6 1.9 %write.1 = (bf16[384,512]{1,0:T(8,128)(2,1)}, bf16[384,512]{1,0:T(8,128)(2,1)}) custom-call(bf16[384,512]{1,0:T(8,128)(2,1)} %get-tuple-element.4.mixer_sum, bf16[384,512]{1,0:T(8,128)(2,1)} %get-tuple-element.5.expert_sum), custom_call_target="tpu_custom_call" | custom-call | tf_op jit(solution)/shard_map/write/pallas_call | solution.py:596

commit v2 on v1

--- a/solution.py
+++ b/solution.py
@@ -128,13 +128,11 @@
     return jnp.dot(a, b, preferred_element_type=F32)
 
 
-def prepare(slot_cap, me, expert_in, expert_gain, ids, weights, own_rows, outgoing, partner_table, combine):
-    tok_dev = expert_in.shape[0]
+def prepare(slot_cap, me, tok_dev, ids, weights, own_table, partner_table, combine):
     picks, all_rows = ids.shape
     blocks = all_rows // tok_dev
     slots = combine.shape[1]
     experts = slots // slot_cap
-    rows = own_rows[...]
     partner = (me + 2) % blocks
     filler = jnp.zeros((8 - 2 * picks, all_rows), F32)
     columns = jnp.transpose(jnp.concatenate([ids[...].astype(F32), weights[...], filler], axis=0))
@@ -163,24 +161,51 @@
         combine[part, :] = mixed
         chosen = jnp.where(me == block, sent, chosen)
         theirs = jnp.where(partner == block, sent, theirs)
-    table = jnp.transpose(chosen).astype(BF16)
+    own_table[...] = jnp.transpose(chosen).astype(BF16).reshape(experts, slot_cap, tok_dev)
     partner_table[...] = jnp.transpose(theirs).astype(BF16).reshape(experts, slot_cap, tok_dev)
-    for expert in range(experts):
-        outgoing[expert] = dot(table[expert * slot_cap : (expert + 1) * slot_cap], rows).astype(BF16)
-
-
-MIX_AT = (0, 3, 4, 5, 8, 9)
-
-LAGS = (0, 1, 2, 4, 5)
+
+
+(
+    SEL, DXW, D2, MIXP, M2S, MIXG, LOADW, MIXPROD, CONV, Q2S, CONVG, PROJ, TAKE, ROWS, EXP, HH, FIN,
+) = range(17)
+
+STEPS = (
+    (SEL, 4), (MIXP, 0), (SEL, 3), (SEL, 2), (M2S, 0), (SEL, 6), (SEL, 0), (DXW, 0),
+    (D2, 1), (TAKE, 3), (SEL, 5), (TAKE, 4), (D2, 3), (TAKE, 6), (TAKE, 0), (SEL, 7),
+    (SEL, 1), (ROWS, 4), (LOADW, 0), (EXP, 4), (MIXG, 0), (ROWS, 6), (TAKE, 5), (EXP, 6),
+    (D2, 2), (MIXPROD, 0), (HH, 4), (D2, 0), (TAKE, 7), (ROWS, 1), (ROWS, 5), (FIN, 4),
+    (ROWS, 0), (CONV, 0), (HH, 6), (EXP, 5), (ROWS, 7), (EXP, 0), (TAKE, 1), (ROWS, 3),
+    (EXP, 7), (FIN, 6), (EXP, 3), (ROWS, 2), (TAKE, 2), (HH, 0), (HH, 5), (EXP, 1),
+    (FIN, 0), (HH, 3), (Q2S, 0), (FIN, 5), (FIN, 3), (EXP, 2), (HH, 7), (HH, 1),
+    (FIN, 7), (FIN, 1), (HH, 2), (FIN, 2), (CONVG, 0), (PROJ, 0),
+)
+
 
 DISP, F2, F1, G1, H2, H1, HG, RET, DISP2 = range(9)
 M2, M1, MG, Q2, Q1, QG, RIM, DX = range(8)
 
 
-def chunk_order(count):
-    half = count // 2
-    far, close = list(range(half, count)), list(range(half))
-    return close[:1] + far + close[1:]
+def looked_up(values, i):
+    bit = 1
+    while len(values) > 1:
+        odd = (i // bit) % 2 == 1
+        values = [
+            jnp.where(odd, pair[-1], pair[0]) if pair[0] is not pair[-1] else pair[0]
+            for pair in (values[n : n + 2] for n in range(0, len(values), 2))
+        ]
+        bit *= 2
+    return values[0]
+
+
+def choose(stage, low, high, bodies):
+    if high - low == 1:
+        bodies[low]()
+        return
+    middle = (low + high) // 2
+    for below in (True, False):
+        @pl.when((stage < middle) if below else (stage >= middle))
+        def _(below=below):
+            choose(stage, *((low, middle) if below else (middle, high)), bodies)
 
 
 def exchange_kernel(
@@ -189,7 +214,7 @@
     mixer_out, expert_out,
     v_in, v_out, v_val, v_proj, v_gate, v_up, v_down,
     v_mixer, v_expert, v_mixer_gain, v_expert_gain, v_ids, v_shares, taps,
-    normed, own_rows, outgoing, partner_table, combine,
+    normed, own_rows, own_table, outgoing, partner_table, combine,
     rows, arrived, hid, res, returned, gates, ext, rim_out, rim_in, gated, dense, outgoing2,
     send, recv, send1, recv1, wsem, fsem,
 ):
@@ -229,14 +254,6 @@
             bit *= 2
         return value
 
-    order = chunk_order(count)
-
-    def shift_of(i):
-        return functools.reduce(jnp.add, [jnp.where(i == n, s, 0) for n, s in enumerate(order)])
-
-    def source_of(i):
-        return mixed_with(shift_of(i))
-
     barrier = pltpu.get_barrier_semaphore()
     for s in range(1, count):
         pl.semaphore_signal(barrier, inc=1, device_id=(mixed_with(s), t), device_id_type=MESH)
@@ -264,88 +281,97 @@
     near, across = (e, t1), (e, t2)
     after = ((e + 1) % count, t)
 
-    def disp(i):
-        return chunk(DISP, i, outgoing.at[source_of(i)], arrived.at[e, t], (source_of(i), t))
-
-    def ret(i):
-        return chunk(RET, i, res.at[source_of(i)], returned.at[e], (source_of(i), t))
-
     def came(kind, i, dst):
         chunk(kind, i, dst, dst, near).wait_recv()
 
     def came_once(kind, dst):
         once(kind, dst, dst, near).wait_recv()
 
+    def disp(i):
+        return chunk(DISP, i, outgoing.at[i], arrived.at[e, t], (mixed_with(i), t))
+
     def disp2(i):
-        src = source_of(i)
-        return chunk(DISP2, i, outgoing2.at[shift_of(i)], arrived.at[e, t2], (src, t))
+        return chunk(DISP2, i, outgoing2.at[i], arrived.at[e, t2], (mixed_with(i), t))
+
+    def ret(i):
+        return chunk(RET, i, res.at[i], returned.at[e], (mixed_with(i), t))
 
     once(DX, own_rows, dense, across).start()
-    prepare(
-        slot_cap, t, v_expert, v_expert_gain, v_ids, v_shares, own_rows, outgoing, partner_table, combine
-    )
-
-    def start_disp(i, carry):
-        @pl.when(shift_of(i) != 0)
-        def _():
+    prepare(slot_cap, t, tok_dev, v_ids, v_shares, own_table, partner_table, combine)
+
+    def sel(i):
+        picked = dot(own_table[mixed_with(i)], own_rows[...]).astype(BF16)
+
+        @pl.when(i == 0)
+        def _():
+            arrived[e, t] = picked
+
+        @pl.when(i != 0)
+        def _():
+            outgoing[i] = picked
             disp(i).start()
 
-        return carry
-
-    lax.fori_loop(0, count, start_disp, 0)
-    for load in firsts[4:]:
-        load.wait()
-    normed[...] = rms_rows(v_mixer[...], v_mixer_gain[...])
-    rows[t] = normed[...]
-    arrived[e, t] = outgoing[e]
-    once(M1, normed, rows.at[t], near).start()
-    came_once(DX, dense)
-
-    def pass_on(i, carry):
-        shift = shift_of(i)
-
-        @pl.when(shift < half)
-        def _():
-            picked = dot(partner_table[source_of(i)], dense[...]).astype(BF16)
-
-            @pl.when(shift == 0)
-            def _():
-                arrived[e, t2] = picked
-
-            @pl.when(shift != 0)
-            def _():
-                outgoing2[shift] = picked
-                disp2(i).start()
-
-        return carry
-
-    lax.fori_loop(0, count, pass_on, 0)
-
-    def finish(i):
-        src = source_of(i)
-        came(H1, i, hid.at[src, t1])
-        came(HG, i, hid.at[src, t3])
-        total = dot(hid[src, 0], v_down[0:hid_width, :])
-        for other in range(1, group):
-            total += dot(hid[src, other], v_down[other * hid_width : (other + 1) * hid_width, :])
-        total = total.astype(BF16).reshape(group, slot_cap, chan)
-
-        @pl.when(shift_of(i) != 0)
-        def _():
-            res[src] = total
-            ret(i).start()
-
-        @pl.when(shift_of(i) == 0)
-        def _():
-            returned[src] = total
-
-    def hand_hidden(i):
-        src = source_of(i)
-        came(H2, i, hid.at[src, t2])
-        chunk(HG, i, hid.at[src, t2], hid.at[src, t2], near).start()
+    def dxw(i):
+        came_once(DX, dense)
+
+    def d2(i):
+        picked = dot(partner_table[mixed_with(i)], dense[...]).astype(BF16)
+
+        @pl.when(i == 0)
+        def _():
+            arrived[e, t2] = picked
+
+        @pl.when(i != 0)
+        def _():
+            outgoing2[i] = picked
+            disp2(i).start()
+
+    def mixp(i):
+        for load in firsts[4:]:
+            load.wait()
+        normed[...] = rms_rows(v_mixer[...], v_mixer_gain[...])
+        rows[t] = normed[...]
+        once(M1, normed, rows.at[t], near).start()
+
+    def m2(i):
+        once(M2, normed, rows.at[t], across).start()
+
+    def mixg(i):
+        came_once(M2, rows.at[t2])
+        once(MG, rows.at[t2], rows.at[t2], near).start()
+
+    def loadw(i):
+        for load in loads:
+            load.wait()
+
+    def take(i):
+        src = mixed_with(i)
+
+        @pl.when(i != 0)
+        def _():
+            came(DISP, i, arrived.at[src, t])
+
+        @pl.when(i >= half)
+        def _():
+            chunk(F2, i, arrived.at[src, t], arrived.at[src, t], across).start()
+
+        chunk(F1, i, arrived.at[src, t], arrived.at[src, t], near).start()
+
+    def hand_rows(i):
+        src = mixed_with(i)
+
+        @pl.when(i >= half)
+        def _():
+            came(F2, i, arrived.at[src, t2])
+
+        @pl.when((i < half) & (i != 0))
+        def _():
+            came(DISP2, i, arrived.at[src, t2])
+
+        chunk(G1, i, arrived.at[src, t2], arrived.at[src, t2], near).start()
 
     def expand(i):
-        src = source_of(i)
+        src = mixed_with(i)
         came(F1, i, arrived.at[src, t1])
         came(G1, i, arrived.at[src, t3])
         x = arrived[src].reshape(group * slot_cap, width)
@@ -355,37 +381,33 @@
         chunk(H2, i, hid.at[src, t], hid.at[src, t], across).start()
         chunk(H1, i, hid.at[src, t], hid.at[src, t], near).start()
 
-    def hand_rows(i):
-        src = source_of(i)
-        shift = shift_of(i)
-
-        @pl.when(shift >= half)
-        def _():
-            came(F2, i, arrived.at[src, t2])
-
-        @pl.when((shift < half) & (shift != 0))
-        def _():
-            came(DISP2, i, arrived.at[src, t2])
-
-        chunk(G1, i, arrived.at[src, t2], arrived.at[src, t2], near).start()
-
-    def take(i):
-        src = source_of(i)
-
-        @pl.when(shift_of(i) != 0)
-        def _():
-            came(DISP, i, arrived.at[src, t])
-
-        @pl.when(shift_of(i) >= half)
-        def _():
-            chunk(F2, i, arrived.at[src, t], arrived.at[src, t], across).start()
-
-        chunk(F1, i, arrived.at[src, t], arrived.at[src, t], near).start()
+    def hand_hidden(i):
+        src = mixed_with(i)
+        came(H2, i, hid.at[src, t2])
+        chunk(HG, i, hid.at[src, t2], hid.at[src, t2], near).start()
+
+    def finish(i):
+        src = mixed_with(i)
+        came(H1, i, hid.at[src, t1])
+        came(HG, i, hid.at[src, t3])
+        total = dot(hid[src, 0], v_down[0:hid_width, :])
+        for other in range(1, group):
+            total += dot(hid[src, other], v_down[other * hid_width : (other + 1) * hid_width, :])
+        total = total.astype(BF16).reshape(group, slot_cap, chan)
+
+        @pl.when(i != 0)
+        def _():
+            res[i] = total
+            ret(i).start()
+
+        @pl.when(i == 0)
+        def _():
+            returned[src] = total
 
     all_rows = group * tok_dev
     tile = 256
 
-    def mixer_products():
+    def mixer_products(i):
         came_once(M1, rows.at[t1])
         came_once(MG, rows.at[t3])
 
@@ -401,7 +423,7 @@
         lax.fori_loop(0, chan // tile, one, 0)
         once(RIM, rim_out, rim_in, after).start()
 
-    def mixer_conv():
+    def mixer_conv(i):
         came_once(RIM, rim_in)
         edge = rim_in[...].astype(F32)[8:16]
         ext[0:8, :] = jnp.where(e == 0, jnp.zeros_like(edge), edge)
@@ -410,10 +432,16 @@
         for n in range(1, tap_count):
             total += taps[n : n + 1, :] * ext[pl.ds(8 - (tap_count - 1) + n, all_rows), :]
         gated[t] = (gates[...] * total).astype(BF16)
+        once(Q1, gated.at[t], gated.at[t], near).start()
+
+    def q2(i):
         once(Q2, gated.at[t], gated.at[t], across).start()
-        once(Q1, gated.at[t], gated.at[t], near).start()
-
-    def mixer_project():
+
+    def convg(i):
+        came_once(Q2, gated.at[t2])
+        once(QG, gated.at[t2], gated.at[t2], near).start()
+
+    def mixer_project(i):
         came_once(Q1, gated.at[t1])
         came_once(QG, gated.at[t3])
 
@@ -427,54 +455,24 @@
 
         lax.fori_loop(0, chan // tile, one, 0)
 
-    stages = (take, hand_rows, expand, hand_hidden, finish)
-
-    def step(i, carry):
-        for stage, lag in reversed(list(zip(stages, LAGS))):
-            @pl.when((i >= lag) & (i < count + lag))
-            def _(stage=stage, lag=lag):
-                stage(i - lag)
-
-        @pl.when(i == MIX_AT[0])
-        def _():
-            once(M2, normed, rows.at[t], across).start()
-            for load in loads:
-                load.wait()
-
-        @pl.when(i == MIX_AT[1])
-        def _():
-            came_once(M2, rows.at[t2])
-            once(MG, rows.at[t2], rows.at[t2], near).start()
-
-        @pl.when(i == MIX_AT[2])
-        def _():
-            mixer_products()
-
-        @pl.when(i == MIX_AT[3])
-        def _():
-            mixer_conv()
-
-        @pl.when(i == MIX_AT[4])
-        def _():
-            came_once(Q2, gated.at[t2])
-            once(QG, gated.at[t2], gated.at[t2], near).start()
-
-        @pl.when(i == MIX_AT[5])
-        def _():
-            mixer_project()
-
+    bodies = (
+        sel, dxw, d2, mixp, m2, mixg, loadw, mixer_products, mixer_conv, q2, convg, mixer_project,
+        take, hand_rows, expand, hand_hidden, finish,
+    )
+    stage_list, shift_list = zip(*STEPS)
+
+    def step(n, carry):
+        stage, shift = looked_up(stage_list, n), looked_up(shift_list, n)
+        choose(stage, 0, len(bodies), [functools.partial(body, shift) for body in bodies])
         return carry
 
-    lax.fori_loop(0, count + LAGS[-1], step, 0)
+    lax.fori_loop(0, len(stage_list), step, 0)
 
     def landed(i, carry):
-        @pl.when(shift_of(i) != 0)
-        def _():
-            came(RET, i, returned.at[source_of(i)])
-
+        came(RET, i, returned.at[mixed_with(i)])
         return carry
 
-    lax.fori_loop(0, count, landed, 0)
+    lax.fori_loop(1, count, landed, 0)
     for block in range(group):
         part = pl.ds(block * tok_dev, tok_dev)
         mix = combine[part, :]
@@ -484,19 +482,19 @@
         expert_out[part, :] = (dot(high, values) + dot(low, values)).astype(BF16)
 
     def drain(i, carry):
-        src = source_of(i)
+        src = mixed_with(i)
         chunk(F1, i, arrived.at[src, t], arrived.at[src, t], near).wait_send()
 
-        @pl.when(shift_of(i) >= half)
+        @pl.when(i >= half)
         def _():
             chunk(F2, i, arrived.at[src, t], arrived.at[src, t], near).wait_send()
 
-        @pl.when(shift_of(i) != 0)
+        @pl.when(i != 0)
         def _():
             disp(i).wait_send()
             ret(i).wait_send()
 
-        @pl.when((shift_of(i) != 0) & (shift_of(i) < half))
+        @pl.when((i != 0) & (i < half))
         def _():
             disp2(i).wait_send()
 
@@ -568,6 +566,7 @@
             pltpu.VMEM((conv_taps.shape[0], chan), F32),
             pltpu.VMEM((tok_dev, width), BF16),
             pltpu.VMEM((tok_dev, width), BF16),
+            pltpu.VMEM((experts, slot_cap, tok_dev), BF16),
             pltpu.VMEM((experts, slot_cap, width), BF16),
             pltpu.VMEM((experts, slot_cap, tok_dev), BF16),
             pltpu.VMEM((all_rows, experts * slot_cap), F32),
@@ -610,7 +609,7 @@
     def body(*args):
         tok_dev, picks, held = args[0].shape[0], args[9].shape[1], args[11].shape[0]
         slot_cap = 2 * tok_dev * picks // (count * held)
-        fits = count in (4, 8, 16) and group == 4 and held == 1 and slot_cap % 16 == 0
+        fits = count == 8 and group == 4 and held == 1 and slot_cap % 16 == 0
         return (fused_on_device if fits and tok_dev % 16 == 0 else on_device)(*args)
 
     return body

time: 94 us -> 85.5 us (0.910)
  Pallas kernels: 92.9 us -> 84.7 us
    pallas_call x1, Pallas kernels: 91 us -> 82.8 us  [fused_on_device(): pl.pallas_call(exchange_kernel, out_shape=(shape((all_rows, chan), BF16),...]
where the time goes in v2:
time: 85.5 us; the launch traced here: 85.4 us
  Pallas kernels  84.7 us (99%)
    pallas_call x1, Pallas kernels, fused_on_device(): pl.pallas_call(exchange_kernel, out_shape=(shape((all_rows, chan), BF16),...  82.8 us
    pallas_call x1, Pallas kernels, fused_on_device(): pl.pallas_call(write_kernel, out_shape=(shape((all_rows, chan), BF16), sh...  1.91 us

profile of v2, /device:TPU:0, one launch (start us, length us, event | category | flops | bytes accessed | tf_op | source)
XLA Modules:
  0.0 85.4 jit_solution(5156322826682225648)
XLA Ops:
  0.6 82.8 %exchange.1 = (bf16[384,512]{1,0:T(8,128)(2,1)}, bf16[384,512]{1,0:T(8,128)(2,1)}) custom-call(bf16[96,2048]{1,0:T(8,128)(2,1)} %mixer_in.1, bf16[96,2048]{1,0:T(8,128)(2,1)} %expert_in.1, f32[1,2048]{1,0:T(1,128)} %bitcast.4, f32[1,2048]{1,0:T(1,128)} %bitcast.5, s32[2,384]{1,0:T(2,128)} %bitcast.6, f32[2,384]{1,0:T(2,128)} %bitcast.7, f32[3,2048]{1,0:T(4,128)} %all_taps.1, ...), custom_call_target="tpu_custom_call" | custom-call | tf_op jit(solution)/shard_map/exchange/pallas_call | solution.py:550
  83.5 1.9 %write.1 = (bf16[384,512]{1,0:T(8,128)(2,1)}, bf16[384,512]{1,0:T(8,128)(2,1)}) custom-call(bf16[384,512]{1,0:T(8,128)(2,1)} %get-tuple-element.4.mixer_sum, bf16[384,512]{1,0:T(8,128)(2,1)} %get-tuple-element.5.expert_sum), custom_call_target="tpu_custom_call" | custom-call | tf_op jit(solution)/shard_map/write/pallas_call | solution.py:595

commit v3 on v2

--- a/solution.py
+++ b/solution.py
@@ -128,61 +128,69 @@
     return jnp.dot(a, b, preferred_element_type=F32)
 
 
-def prepare(slot_cap, me, tok_dev, ids, weights, own_table, partner_table, combine):
+def fill_columns(ids, weights, columns):
     picks, all_rows = ids.shape
-    blocks = all_rows // tok_dev
-    slots = combine.shape[1]
-    experts = slots // slot_cap
-    partner = (me + 2) % blocks
     filler = jnp.zeros((8 - 2 * picks, all_rows), F32)
-    columns = jnp.transpose(jnp.concatenate([ids[...].astype(F32), weights[...], filler], axis=0))
+    columns[...] = jnp.transpose(jnp.concatenate([ids[...].astype(F32), weights[...], filler], axis=0))
+
+
+def placed(columns, block, tok_dev, picks, slots, slot_cap, shared):
+    own = columns[pl.ds(pl.multiple_of(block * tok_dev, tok_dev), tok_dev), :]
     below = (
         lax.broadcasted_iota(jnp.int32, (tok_dev, tok_dev), 1)
         < lax.broadcasted_iota(jnp.int32, (tok_dev, tok_dev), 0)
     ).astype(BF16)
     labels = lax.broadcasted_iota(jnp.int32, (tok_dev, 128), 1)
     places = lax.broadcasted_iota(jnp.int32, (tok_dev, slots), 1)
-    chosen = jnp.zeros((tok_dev, slots), F32)
-    theirs = jnp.zeros((tok_dev, slots), F32)
-    for block in range(blocks):
-        part = slice(block * tok_dev, (block + 1) * tok_dev)
-        named = [columns[part, k : k + 1].astype(jnp.int32) for k in range(picks)]
-        share = [columns[part, picks + k : picks + k + 1] for k in range(picks)]
-        total = functools.reduce(jnp.add, share)
-        hot = [(labels == n).astype(F32) for n in named]
-        rank = dot(below, functools.reduce(jnp.add, hot).astype(BF16))
-        mixed = jnp.zeros((tok_dev, slots), F32)
-        sent = jnp.zeros((tok_dev, slots), F32)
-        for k in range(picks):
-            within = jnp.sum(rank * hot[k], axis=1, keepdims=True).astype(jnp.int32)
-            spot = places == named[k] * slot_cap + within
-            mixed = mixed + jnp.where(spot, share[k] / total, 0.0)
-            sent = sent + jnp.where(spot, 1.0, 0.0)
-        combine[part, :] = mixed
-        chosen = jnp.where(me == block, sent, chosen)
-        theirs = jnp.where(partner == block, sent, theirs)
-    own_table[...] = jnp.transpose(chosen).astype(BF16).reshape(experts, slot_cap, tok_dev)
-    partner_table[...] = jnp.transpose(theirs).astype(BF16).reshape(experts, slot_cap, tok_dev)
+    named = [own[:, k : k + 1].astype(jnp.int32) for k in range(picks)]
+    share = [own[:, picks + k : picks + k + 1] for k in range(picks)]
+    total = functools.reduce(jnp.add, share)
+    hot = [(labels == n).astype(F32) for n in named]
+    rank = dot(below, functools.reduce(jnp.add, hot).astype(BF16))
+    result = jnp.zeros((tok_dev, slots), F32)
+    for k in range(picks):
+        within = jnp.sum(rank * hot[k], axis=1, keepdims=True).astype(jnp.int32)
+        spot = places == named[k] * slot_cap + within
+        result = result + jnp.where(spot, share[k] / total if shared else 1.0, 0.0)
+    return result
 
 
 (
-    SEL, DXW, D2, MIXP, M2S, MIXG, LOADW, MIXPROD, CONV, Q2S, CONVG, PROJ, TAKE, ROWS, EXP, HH, FIN,
-) = range(17)
-
-STEPS = (
-    (SEL, 4), (MIXP, 0), (SEL, 3), (SEL, 2), (M2S, 0), (SEL, 6), (SEL, 0), (DXW, 0),
-    (D2, 1), (TAKE, 3), (SEL, 5), (TAKE, 4), (D2, 3), (TAKE, 6), (TAKE, 0), (SEL, 7),
-    (SEL, 1), (ROWS, 4), (LOADW, 0), (EXP, 4), (MIXG, 0), (ROWS, 6), (TAKE, 5), (EXP, 6),
-    (D2, 2), (MIXPROD, 0), (HH, 4), (D2, 0), (TAKE, 7), (ROWS, 1), (ROWS, 5), (FIN, 4),
-    (ROWS, 0), (CONV, 0), (HH, 6), (EXP, 5), (ROWS, 7), (EXP, 0), (TAKE, 1), (ROWS, 3),
-    (EXP, 7), (FIN, 6), (EXP, 3), (ROWS, 2), (TAKE, 2), (HH, 0), (HH, 5), (EXP, 1),
-    (FIN, 0), (HH, 3), (Q2S, 0), (FIN, 5), (FIN, 3), (EXP, 2), (HH, 7), (HH, 1),
-    (FIN, 7), (FIN, 1), (HH, 2), (FIN, 2), (CONVG, 0), (PROJ, 0),
+    SEL, DXW, D2, PTAB, COMB, MIXP, M2S, MIXG, LOADW, MIXPROD, CONV, Q2S, CONVG, PROJ,
+    TAKE, ROWS, EXP, HH, FIN, REST,
+) = range(20)
+
+PIECES = 4
+
+END_STEPS = (
+    (SEL, 7), (MIXP, 0), (SEL, 2), (SEL, 5), (TAKE, 7), (PTAB, 0), (SEL, 0),
+    (TAKE, 3), (M2S, 2), (M2S, 1), (SEL, 1), (TAKE, 0), (DXW, 0), (D2, 1),
+    (M2S, 0), (M2S, 3), (D2, 2), (ROWS, 7), (SEL, 6), (COMB, 0), (LOADW, 0),
+    (EXP, 7), (TAKE, 1), (SEL, 4), (SEL, 3), (TAKE, 2), (D2, 0), (TAKE, 4),
+    (D2, 3), (MIXG, 0), (MIXPROD, 0), (HH, 7), (TAKE, 6), (FIN, 7), (TAKE, 5),
+    (ROWS, 6), (CONV, 0), (ROWS, 3), (ROWS, 4), (ROWS, 1), (EXP, 6), (EXP, 4),
+    (ROWS, 5), (ROWS, 0), (EXP, 5), (EXP, 3), (HH, 6), (ROWS, 2), (FIN, 6),
+    (EXP, 1), (EXP, 2), (HH, 5), (FIN, 5), (Q2S, 2), (HH, 4), (HH, 1),
+    (HH, 2), (Q2S, 3), (FIN, 4), (HH, 3), (FIN, 1), (Q2S, 1), (EXP, 0),
+    (FIN, 2), (Q2S, 0), (HH, 0), (FIN, 3), (CONVG, 0), (FIN, 0), (PROJ, 0),
 )
 
-
-DISP, F2, F1, G1, H2, H1, HG, RET, DISP2 = range(9)
-M2, M1, MG, Q2, Q1, QG, RIM, DX = range(8)
+MIDDLE_STEPS = (
+    (SEL, 7), (SEL, 3), (SEL, 2), (MIXP, 0), (M2S, 2), (SEL, 1), (M2S, 0),
+    (M2S, 3), (SEL, 4), (PTAB, 0), (DXW, 0), (D2, 3), (M2S, 1), (TAKE, 7),
+    (SEL, 0), (TAKE, 0), (D2, 0), (D2, 1), (TAKE, 2), (SEL, 5), (TAKE, 5),
+    (ROWS, 2), (ROWS, 7), (MIXG, 0), (COMB, 0), (LOADW, 0), (EXP, 2), (SEL, 6),
+    (EXP, 7), (ROWS, 5), (TAKE, 4), (MIXPROD, 0), (HH, 2), (ROWS, 1), (EXP, 5),
+    (HH, 7), (D2, 2), (FIN, 7), (CONV, 0), (TAKE, 3), (TAKE, 1), (ROWS, 0),
+    (Q2S, 1), (ROWS, 4), (FIN, 2), (HH, 5), (ROWS, 3), (TAKE, 6), (EXP, 4),
+    (EXP, 3), (Q2S, 0), (FIN, 5), (EXP, 0), (EXP, 1), (Q2S, 2), (HH, 4),
+    (HH, 3), (ROWS, 6), (FIN, 3), (FIN, 4), (HH, 1), (EXP, 6), (FIN, 1),
+    (HH, 0), (FIN, 0), (Q2S, 3), (HH, 6), (FIN, 6), (CONVG, 0), (PROJ, 0),
+)
+
+
+DISP, F2, F1, G1, H2, H1, HG, RET, DISP2, M2, Q2 = range(11)
+M1, MG, Q1, QG, RIM, DX = range(6)
 
 
 def looked_up(values, i):
@@ -214,13 +222,14 @@
     mixer_out, expert_out,
     v_in, v_out, v_val, v_proj, v_gate, v_up, v_down,
     v_mixer, v_expert, v_mixer_gain, v_expert_gain, v_ids, v_shares, taps,
-    normed, own_rows, own_table, outgoing, partner_table, combine,
+    columns, normed, own_rows, own_table, outgoing, partner_table, combine,
     rows, arrived, hid, res, returned, gates, ext, rim_out, rim_in, gated, dense, outgoing2,
     send, recv, send1, recv1, wsem, fsem,
 ):
     count = outgoing.shape[0]
     group, tok_dev, width = rows.shape
     half = count // 2
+    all_rows = group * tok_dev
     chan = v_in.shape[1]
     slot_cap = outgoing.shape[1]
     hid_width = v_gate.shape[1]
@@ -263,7 +272,16 @@
         load.wait()
     for load in loads:
         load.start()
+    picks = v_ids.shape[0]
+    slots = combine.shape[1]
+
+    def table_of(block):
+        sent = placed(columns, block, tok_dev, picks, slots, slot_cap, False)
+        return jnp.transpose(sent).astype(BF16).reshape(slots // slot_cap, slot_cap, tok_dev)
+
     own_rows[...] = rms_rows(v_expert[...], v_expert_gain[...])
+    fill_columns(v_ids, v_shares, columns)
+    own_table[...] = table_of(t)
     pl.semaphore_wait(barrier, count + 1)
 
     def chunk(kind, i, src, dst, dev):
@@ -297,7 +315,6 @@
         return chunk(RET, i, res.at[i], returned.at[e], (mixed_with(i), t))
 
     once(DX, own_rows, dense, across).start()
-    prepare(slot_cap, t, tok_dev, v_ids, v_shares, own_table, partner_table, combine)
 
     def sel(i):
         picked = dot(own_table[mixed_with(i)], own_rows[...]).astype(BF16)
@@ -333,11 +350,31 @@
         rows[t] = normed[...]
         once(M1, normed, rows.at[t], near).start()
 
+    def ptab(i):
+        partner_table[...] = table_of(t2)
+
+    def comb(i):
+        def one(block, carry):
+            part = pl.ds(pl.multiple_of(block * tok_dev, tok_dev), tok_dev)
+            combine[part, :] = placed(columns, block, tok_dev, picks, slots, slot_cap, True)
+            return carry
+
+        lax.fori_loop(0, group, one, 0)
+
+    def m2_piece(i, home, dev):
+        cols = pl.ds(pl.multiple_of(i * (width // PIECES), 128), width // PIECES)
+        return chunk(M2, i, normed.at[:, cols], rows.at[home, :, cols], dev)
+
+    def q2_piece(i, home, dev):
+        part = pl.ds(pl.multiple_of(i * (all_rows // PIECES), 16), all_rows // PIECES)
+        return chunk(Q2, i, gated.at[home, part], gated.at[home, part], dev)
+
     def m2(i):
-        once(M2, normed, rows.at[t], across).start()
+        m2_piece(i, t, across).start()
 
     def mixg(i):
-        came_once(M2, rows.at[t2])
+        for n in range(PIECES):
+            m2_piece(n, t2, near).wait_recv()
         once(MG, rows.at[t2], rows.at[t2], near).start()
 
     def loadw(i):
@@ -404,7 +441,6 @@
         def _():
             returned[src] = total
 
-    all_rows = group * tok_dev
     tile = 256
 
     def mixer_products(i):
@@ -435,10 +471,11 @@
         once(Q1, gated.at[t], gated.at[t], near).start()
 
     def q2(i):
-        once(Q2, gated.at[t], gated.at[t], across).start()
+        q2_piece(i, t, across).start()
 
     def convg(i):
-        came_once(Q2, gated.at[t2])
+        for n in range(PIECES):
+            q2_piece(n, t2, near).wait_recv()
         once(QG, gated.at[t2], gated.at[t2], near).start()
 
     def mixer_project(i):
@@ -455,18 +492,24 @@
 
         lax.fori_loop(0, chan // tile, one, 0)
 
+    def rest(i):
+        pass
+
     bodies = (
-        sel, dxw, d2, mixp, m2, mixg, loadw, mixer_products, mixer_conv, q2, convg, mixer_project,
-        take, hand_rows, expand, hand_hidden, finish,
-    )
-    stage_list, shift_list = zip(*STEPS)
+        sel, dxw, d2, ptab, comb, mixp, m2, mixg, loadw, mixer_products, mixer_conv, q2, convg, mixer_project,
+        take, hand_rows, expand, hand_hidden, finish, rest,
+    )
+    middle = (e >= count // 4) & (e < 3 * count // 4)
+    steps = max(len(END_STEPS), len(MIDDLE_STEPS))
+    tables = [table + ((REST, 0),) * (steps - len(table)) for table in (END_STEPS, MIDDLE_STEPS)]
 
     def step(n, carry):
-        stage, shift = looked_up(stage_list, n), looked_up(shift_list, n)
+        at = [[looked_up(list(part), n) for part in zip(*table)] for table in tables]
+        stage, shift = [jnp.where(middle, inner, outer) for outer, inner in zip(*at)]
         choose(stage, 0, len(bodies), [functools.partial(body, shift) for body in bodies])
         return carry
 
-    lax.fori_loop(0, len(stage_list), step, 0)
+    lax.fori_loop(0, steps, step, 0)
 
     def landed(i, carry):
         came(RET, i, returned.at[mixed_with(i)])
@@ -505,12 +548,13 @@
         return carry
 
     lax.fori_loop(0, count, drain, 0)
-    for kind in (M2, M1):
-        once(kind, normed, rows.at[t], near).wait_send()
+    once(M1, normed, rows.at[t], near).wait_send()
+    for n in range(PIECES):
+        m2_piece(n, t, near).wait_send()
+        q2_piece(n, t, near).wait_send()
     once(MG, rows.at[t2], rows.at[t2], near).wait_send()
     once(DX, own_rows, dense, near).wait_send()
-    for kind in (Q2, Q1):
-        once(kind, gated.at[t], gated.at[t], near).wait_send()
+    once(Q1, gated.at[t], gated.at[t], near).wait_send()
     once(QG, gated.at[t2], gated.at[t2], near).wait_send()
     once(RIM, rim_out, rim_in, after).wait_send()
 
@@ -564,6 +608,7 @@
             pltpu.VMEM(route_ids.shape[::-1], jnp.int32),
             pltpu.VMEM(route_ids.shape[::-1], F32),
             pltpu.VMEM((conv_taps.shape[0], chan), F32),
+            pltpu.VMEM((all_rows, 8), F32),
             pltpu.VMEM((tok_dev, width), BF16),
             pltpu.VMEM((tok_dev, width), BF16),
             pltpu.VMEM((experts, slot_cap, tok_dev), BF16),
@@ -582,7 +627,7 @@
             pltpu.VMEM((group, all_rows, chan), BF16),
             pltpu.VMEM((tok_dev, width), BF16),
             pltpu.VMEM((count // 2, slot_cap, width), BF16),
-            dma((9, count)), dma((9, count)), dma((8,)), dma((8,)), dma((7,)), dma((7,)),
+            dma((11, count)), dma((11, count)), dma((6,)), dma((6,)), dma((7,)), dma((7,)),
         ],
         compiler_params=pltpu.CompilerParams(
             collective_id=0, has_side_effects=True, vmem_limit_bytes=VMEM_BYTES

time: 85.5 us -> 81 us (0.947)
  Pallas kernels: 84.7 us -> 80 us
    pallas_call x1, Pallas kernels: 82.8 us -> 78.1 us  [fused_on_device(): pl.pallas_call(exchange_kernel, out_shape=(shape((all_rows, chan), BF16),...]
where the time goes in v3:
time: 81 us; the launch traced here: 80.7 us
  Pallas kernels  80 us (99%)
    pallas_call x1, Pallas kernels, fused_on_device(): pl.pallas_call(exchange_kernel, out_shape=(shape((all_rows, chan), BF16),...  78.1 us
    pallas_call x1, Pallas kernels, fused_on_device(): pl.pallas_call(write_kernel, out_shape=(shape((all_rows, chan), BF16), sh...  1.91 us

profile of v3, /device:TPU:0, one launch (start us, length us, event | category | flops | bytes accessed | tf_op | source)
XLA Modules:
  0.0 80.7 jit_solution(1178116908227841402)
XLA Ops:
  0.6 78.1 %exchange.1 = (bf16[384,512]{1,0:T(8,128)(2,1)}, bf16[384,512]{1,0:T(8,128)(2,1)}) custom-call(bf16[96,2048]{1,0:T(8,128)(2,1)} %mixer_in.1, bf16[96,2048]{1,0:T(8,128)(2,1)} %expert_in.1, f32[1,2048]{1,0:T(1,128)} %bitcast.4, f32[1,2048]{1,0:T(1,128)} %bitcast.5, s32[2,384]{1,0:T(2,128)} %bitcast.6, f32[2,384]{1,0:T(2,128)} %bitcast.7, f32[3,2048]{1,0:T(4,128)} %all_taps.1, ...), custom_call_target="tpu_custom_call" | custom-call | tf_op jit(solution)/shard_map/exchange/pallas_call | solution.py:594
  78.8 1.9 %write.1 = (bf16[384,512]{1,0:T(8,128)(2,1)}, bf16[384,512]{1,0:T(8,128)(2,1)}) custom-call(bf16[384,512]{1,0:T(8,128)(2,1)} %get-tuple-element.4.mixer_sum, bf16[384,512]{1,0:T(8,128)(2,1)} %get-tuple-element.5.expert_sum), custom_call_target="tpu_custom_call" | custom-call | tf_op jit(solution)/shard_map/write/pallas_call | solution.py:640

commit v4 on v3

--- a/solution.py
+++ b/solution.py
@@ -128,10 +128,11 @@
     return jnp.dot(a, b, preferred_element_type=F32)
 
 
-def fill_columns(ids, weights, columns):
+def fill_columns(ids, weights, routes, columns):
     picks, all_rows = ids.shape
     filler = jnp.zeros((8 - 2 * picks, all_rows), F32)
-    columns[...] = jnp.transpose(jnp.concatenate([ids[...].astype(F32), weights[...], filler], axis=0))
+    routes[...] = jnp.concatenate([ids[...].astype(F32), weights[...], filler], axis=0)
+    columns[...] = jnp.transpose(routes[...])
 
 
 def placed(columns, block, tok_dev, picks, slots, slot_cap, shared):
@@ -157,39 +158,42 @@
 
 (
     SEL, DXW, D2, PTAB, COMB, MIXP, M2S, MIXG, LOADW, MIXPROD, CONV, Q2S, CONVG, PROJ,
-    TAKE, ROWS, EXP, HH, FIN, REST,
-) = range(20)
+    TAKE, ROWS, EXP, HH, FIN, REST, FARW, GSEL,
+) = range(22)
 
 PIECES = 4
 
+GATES = (4,)
+
 END_STEPS = (
-    (SEL, 7), (MIXP, 0), (SEL, 2), (SEL, 5), (TAKE, 7), (PTAB, 0), (SEL, 0),
-    (TAKE, 3), (M2S, 2), (M2S, 1), (SEL, 1), (TAKE, 0), (DXW, 0), (D2, 1),
-    (M2S, 0), (M2S, 3), (D2, 2), (ROWS, 7), (SEL, 6), (COMB, 0), (LOADW, 0),
-    (EXP, 7), (TAKE, 1), (SEL, 4), (SEL, 3), (TAKE, 2), (D2, 0), (TAKE, 4),
-    (D2, 3), (MIXG, 0), (MIXPROD, 0), (HH, 7), (TAKE, 6), (FIN, 7), (TAKE, 5),
-    (ROWS, 6), (CONV, 0), (ROWS, 3), (ROWS, 4), (ROWS, 1), (EXP, 6), (EXP, 4),
-    (ROWS, 5), (ROWS, 0), (EXP, 5), (EXP, 3), (HH, 6), (ROWS, 2), (FIN, 6),
-    (EXP, 1), (EXP, 2), (HH, 5), (FIN, 5), (Q2S, 2), (HH, 4), (HH, 1),
-    (HH, 2), (Q2S, 3), (FIN, 4), (HH, 3), (FIN, 1), (Q2S, 1), (EXP, 0),
-    (FIN, 2), (Q2S, 0), (HH, 0), (FIN, 3), (CONVG, 0), (FIN, 0), (PROJ, 0),
+    (PTAB, 0), (MIXP, 0), (TAKE, 3), (M2S, 3), (SEL, 2), (M2S, 2), (M2S, 1),
+    (TAKE, 4), (SEL, 1), (DXW, 0), (D2, 2), (M2S, 0), (ROWS, 4), (D2, 1),
+    (ROWS, 3), (COMB, 0), (D2, 3), (LOADW, 0), (EXP, 4), (SEL, 3), (TAKE, 5),
+    (MIXG, 0), (HH, 4), (TAKE, 7), (FIN, 4), (ROWS, 5), (TAKE, 6), (MIXPROD, 0),
+    (ROWS, 7), (EXP, 5), (ROWS, 1), (ROWS, 2), (CONV, 0), (EXP, 7), (SEL, 0),
+    (ROWS, 6), (EXP, 3), (D2, 0), (TAKE, 1), (EXP, 6), (ROWS, 0), (Q2S, 2),
+    (HH, 7), (Q2S, 3), (FIN, 7), (TAKE, 0), (Q2S, 0), (HH, 3), (HH, 6),
+    (TAKE, 2), (EXP, 1), (FIN, 6), (HH, 5), (EXP, 2), (FIN, 3), (Q2S, 1),
+    (EXP, 0), (FIN, 5), (HH, 1), (HH, 2), (CONVG, 0), (FIN, 1), (FIN, 2),
+    (PROJ, 0), (HH, 0), (FIN, 0),
 )
 
 MIDDLE_STEPS = (
-    (SEL, 7), (SEL, 3), (SEL, 2), (MIXP, 0), (M2S, 2), (SEL, 1), (M2S, 0),
-    (M2S, 3), (SEL, 4), (PTAB, 0), (DXW, 0), (D2, 3), (M2S, 1), (TAKE, 7),
-    (SEL, 0), (TAKE, 0), (D2, 0), (D2, 1), (TAKE, 2), (SEL, 5), (TAKE, 5),
-    (ROWS, 2), (ROWS, 7), (MIXG, 0), (COMB, 0), (LOADW, 0), (EXP, 2), (SEL, 6),
-    (EXP, 7), (ROWS, 5), (TAKE, 4), (MIXPROD, 0), (HH, 2), (ROWS, 1), (EXP, 5),
-    (HH, 7), (D2, 2), (FIN, 7), (CONV, 0), (TAKE, 3), (TAKE, 1), (ROWS, 0),
-    (Q2S, 1), (ROWS, 4), (FIN, 2), (HH, 5), (ROWS, 3), (TAKE, 6), (EXP, 4),
-    (EXP, 3), (Q2S, 0), (FIN, 5), (EXP, 0), (EXP, 1), (Q2S, 2), (HH, 4),
-    (HH, 3), (ROWS, 6), (FIN, 3), (FIN, 4), (HH, 1), (EXP, 6), (FIN, 1),
-    (HH, 0), (FIN, 0), (Q2S, 3), (HH, 6), (FIN, 6), (CONVG, 0), (PROJ, 0),
+    (SEL, 4), (SEL, 3), (MIXP, 0), (PTAB, 0), (M2S, 3), (SEL, 1), (SEL, 7),
+    (COMB, 0), (SEL, 5), (DXW, 0), (D2, 3), (M2S, 1), (M2S, 0), (FARW, 4),
+    (GSEL, 4), (GSEL, 5), (TAKE, 4), (TAKE, 1), (TAKE, 7), (D2, 1), (ROWS, 4),
+    (D2, 0), (GSEL, 7), (LOADW, 0), (EXP, 4), (SEL, 6), (SEL, 0), (M2S, 2),
+    (ROWS, 7), (GSEL, 6), (D2, 2), (EXP, 7), (TAKE, 5), (MIXG, 0), (MIXPROD, 0),
+    (TAKE, 3), (HH, 4), (TAKE, 6), (HH, 7), (ROWS, 0), (ROWS, 2), (ROWS, 3),
+    (TAKE, 2), (FIN, 4), (ROWS, 1), (FIN, 7), (EXP, 1), (EXP, 3), (SEL, 2),
+    (ROWS, 6), (CONV, 0), (ROWS, 5), (EXP, 2), (HH, 3), (TAKE, 0), (EXP, 5),
+    (EXP, 0), (EXP, 6), (HH, 1), (Q2S, 2), (HH, 0), (HH, 5), (FIN, 3),
+    (Q2S, 0), (Q2S, 3), (HH, 2), (Q2S, 1), (FIN, 1), (FIN, 5), (FIN, 2),
+    (FIN, 0), (HH, 6), (FIN, 6), (CONVG, 0), (PROJ, 0),
 )
 
 
-DISP, F2, F1, G1, H2, H1, HG, RET, DISP2, M2, Q2 = range(11)
+DISP, F2, F1, G1, H2, H1, HG, RET, DISP2, M2, Q2, FARR, FARI, GD = range(14)
 M1, MG, Q1, QG, RIM, DX = range(6)
 
 
@@ -223,7 +227,7 @@
     v_in, v_out, v_val, v_proj, v_gate, v_up, v_down,
     v_mixer, v_expert, v_mixer_gain, v_expert_gain, v_ids, v_shares, taps,
     columns, normed, own_rows, own_table, outgoing, partner_table, combine,
-    rows, arrived, hid, res, returned, gates, ext, rim_out, rim_in, gated, dense, outgoing2,
+    rows, arrived, hid, res, returned, gates, ext, rim_out, rim_in, gated, dense, outgoing2, routes, far_rows, far_routes, far_columns, far_tables, far_out,
     send, recv, send1, recv1, wsem, fsem,
 ):
     count = outgoing.shape[0]
@@ -256,12 +260,17 @@
              (w_up.at[0], v_up), (w_down.at[0], v_down), (w_proj, v_proj)]
         )
     ]
-    def mixed_with(s):
+    def xor(a, b):
         value, bit = 0, 1
         while bit < count:
-            value = value + ((e // bit + s // bit) % 2) * bit
+            value = value + ((a // bit + b // bit) % 2) * bit
             bit *= 2
         return value
+
+    def mixed_with(s):
+        return xor(e, s)
+
+    middle = (e >= count // 4) & (e < 3 * count // 4)
 
     barrier = pltpu.get_barrier_semaphore()
     for s in range(1, count):
@@ -275,13 +284,13 @@
     picks = v_ids.shape[0]
     slots = combine.shape[1]
 
-    def table_of(block):
-        sent = placed(columns, block, tok_dev, picks, slots, slot_cap, False)
+    def table_of(source, block):
+        sent = placed(source, block, tok_dev, picks, slots, slot_cap, False)
         return jnp.transpose(sent).astype(BF16).reshape(slots // slot_cap, slot_cap, tok_dev)
 
     own_rows[...] = rms_rows(v_expert[...], v_expert_gain[...])
-    fill_columns(v_ids, v_shares, columns)
-    own_table[...] = table_of(t)
+    fill_columns(v_ids, v_shares, routes, columns)
+    own_table[...] = table_of(columns, t)
     pl.semaphore_wait(barrier, count + 1)
 
     def chunk(kind, i, src, dst, dev):
@@ -314,7 +323,60 @@
     def ret(i):
         return chunk(RET, i, res.at[i], returned.at[e], (mixed_with(i), t))
 
+    def far_pair(gate):
+        dev = (mixed_with(gate), t)
+        slot = GATES.index(gate)
+        return (
+            chunk(FARR, slot, own_rows, far_rows.at[slot], dev),
+            chunk(FARI, slot, routes, far_routes.at[slot], dev),
+        )
+
+    def for_far(act):
+        for gate in GATES:
+            @pl.when(middle if gate == count - 2 else ~middle)
+            def _(gate=gate):
+                for copy in far_pair(gate):
+                    act(copy)
+
+    for_far(lambda copy: copy.start())
     once(DX, own_rows, dense, across).start()
+
+    def farw(i):
+        slot = (i - half) // 2 if len(GATES) > 1 else 0
+        for copy in (
+            chunk(FARR, slot, far_rows.at[slot], far_rows.at[slot], near),
+            chunk(FARI, slot, far_routes.at[slot], far_routes.at[slot], near),
+        ):
+            copy.wait_recv()
+        far_columns[...] = jnp.transpose(far_routes[slot])
+        far_tables[slot] = table_of(far_columns, t)
+
+    def passed(i):
+        gate = jnp.where(i >= count, GATES[-1], GATES[0])
+        slot = i // count
+        shift = i % count
+        return gate, slot, shift, xor(mixed_with(gate), shift)
+
+    def gsend(i):
+        gate, slot, shift, expert = passed(i)
+        return pltpu.make_async_remote_copy(
+            src_ref=far_out.at[slot, shift - half], dst_ref=arrived.at[mixed_with(gate), t],
+            send_sem=send.at[GD, slot * half + shift - half], recv_sem=recv.at[DISP, shift],
+            device_id=(expert, t), device_id_type=MESH,
+        )
+
+    def gsel(i):
+        gate, slot, shift, expert = passed(i)
+        picked = dot(far_tables[slot, expert], far_rows[slot]).astype(BF16)
+
+        @pl.when(shift == gate)
+        def _():
+            arrived[mixed_with(gate), t] = picked
+
+        @pl.when(shift != gate)
+        def _():
+            far_out[slot, shift - half] = picked
+            gsend(i).start()
 
     def sel(i):
         picked = dot(own_table[mixed_with(i)], own_rows[...]).astype(BF16)
@@ -351,7 +413,7 @@
         once(M1, normed, rows.at[t], near).start()
 
     def ptab(i):
-        partner_table[...] = table_of(t2)
+        partner_table[...] = table_of(columns, t2)
 
     def comb(i):
         def one(block, carry):
@@ -383,8 +445,11 @@
 
     def take(i):
         src = mixed_with(i)
-
-        @pl.when(i != 0)
+        here = i == 0
+        for gate in GATES:
+            here = here | (middle & (i == gate))
+
+        @pl.when(~here)
         def _():
             came(DISP, i, arrived.at[src, t])
 
@@ -497,9 +562,8 @@
 
     bodies = (
         sel, dxw, d2, ptab, comb, mixp, m2, mixg, loadw, mixer_products, mixer_conv, q2, convg, mixer_project,
-        take, hand_rows, expand, hand_hidden, finish, rest,
-    )
-    middle = (e >= count // 4) & (e < 3 * count // 4)
+        take, hand_rows, expand, hand_hidden, finish, rest, farw, gsel,
+    )
     steps = max(len(END_STEPS), len(MIDDLE_STEPS))
     tables = [table + ((REST, 0),) * (steps - len(table)) for table in (END_STEPS, MIDDLE_STEPS)]
 
@@ -534,8 +598,13 @@
 
         @pl.when(i != 0)
         def _():
+            ret(i).wait_send()
+
+        direct = (i < half) | jnp.where(middle, True, False)
+
+        @pl.when((i != 0) & direct)
+        def _():
             disp(i).wait_send()
-            ret(i).wait_send()
 
         @pl.when((i != 0) & (i < half))
         def _():
@@ -548,6 +617,15 @@
         return carry
 
     lax.fori_loop(0, count, drain, 0)
+    for_far(lambda copy: copy.wait_send())
+
+    @pl.when(middle)
+    def _():
+        for slot, gate in enumerate(GATES):
+            for shift in range(half, count):
+                if shift != gate:
+                    gsend(slot * count + shift).wait_send()
+
     once(M1, normed, rows.at[t], near).wait_send()
     for n in range(PIECES):
         m2_piece(n, t, near).wait_send()
@@ -627,7 +705,13 @@
             pltpu.VMEM((group, all_rows, chan), BF16),
             pltpu.VMEM((tok_dev, width), BF16),
             pltpu.VMEM((count // 2, slot_cap, width), BF16),
-            dma((11, count)), dma((11, count)), dma((6,)), dma((6,)), dma((7,)), dma((7,)),
+            pltpu.VMEM((8, all_rows), F32),
+            pltpu.VMEM((len(GATES), tok_dev, width), BF16),
+            pltpu.VMEM((len(GATES), 8, all_rows), F32),
+            pltpu.VMEM((all_rows, 8), F32),
+            pltpu.VMEM((len(GATES), experts, slot_cap, tok_dev), BF16),
+            pltpu.VMEM((len(GATES), count // 2, slot_cap, width), BF16),
+            dma((14, count)), dma((14, count)), dma((6,)), dma((6,)), dma((7,)), dma((7,)),
         ],
         compiler_params=pltpu.CompilerParams(
             collective_id=0, has_side_effects=True, vmem_limit_bytes=VMEM_BYTES

time: 81 us -> 83.6 us (1.032)
  Pallas kernels: 80 us -> 82.8 us
    pallas_call x1, Pallas kernels: 78.1 us -> 80.9 us  [fused_on_device(): pl.pallas_call(exchange_kernel, out_shape=(shape((all_rows, chan), BF16),...]
where the time goes in v4:
time: 83.6 us; the launch traced here: 83.4 us
  Pallas kernels  82.8 us (99%)
    pallas_call x1, Pallas kernels, fused_on_device(): pl.pallas_call(exchange_kernel, out_shape=(shape((all_rows, chan), BF16),...  80.9 us
    pallas_call x1, Pallas kernels, fused_on_device(): pl.pallas_call(write_kernel, out_shape=(shape((all_rows, chan), BF16), sh...  1.91 us

profile of v4, /device:TPU:0, one launch (start us, length us, event | category | flops | bytes accessed | tf_op | source)
XLA Modules:
  0.0 83.4 jit_solution(13707430045053940828)
XLA Ops:
  0.6 80.9 %exchange.1 = (bf16[384,512]{1,0:T(8,128)(2,1)}, bf16[384,512]{1,0:T(8,128)(2,1)}) custom-call(bf16[96,2048]{1,0:T(8,128)(2,1)} %mixer_in.1, bf16[96,2048]{1,0:T(8,128)(2,1)} %expert_in.1, f32[1,2048]{1,0:T(1,128)} %bitcast.4, f32[1,2048]{1,0:T(1,128)} %bitcast.5, s32[2,384]{1,0:T(2,128)} %bitcast.6, f32[2,384]{1,0:T(2,128)} %bitcast.7, f32[3,2048]{1,0:T(4,128)} %all_taps.1, ...), custom_call_target="tpu_custom_call" | custom-call | tf_op jit(solution)/shard_map/exchange/pallas_call | solution.py:672
  81.5 1.9 %write.1 = (bf16[384,512]{1,0:T(8,128)(2,1)}, bf16[384,512]{1,0:T(8,128)(2,1)}) custom-call(bf16[384,512]{1,0:T(8,128)(2,1)} %get-tuple-element.4.mixer_sum, bf16[384,512]{1,0:T(8,128)(2,1)} %get-tuple-element.5.expert_sum), custom_call_target="tpu_custom_call" | custom-call | tf_op jit(solution)/shard_map/write/pallas_call | solution.py:724

commit v5 on v4

--- a/solution.py
+++ b/solution.py
@@ -163,33 +163,33 @@
 
 PIECES = 4
 
-GATES = (4,)
+GATES = (6,)
 
 END_STEPS = (
-    (PTAB, 0), (MIXP, 0), (TAKE, 3), (M2S, 3), (SEL, 2), (M2S, 2), (M2S, 1),
-    (TAKE, 4), (SEL, 1), (DXW, 0), (D2, 2), (M2S, 0), (ROWS, 4), (D2, 1),
-    (ROWS, 3), (COMB, 0), (D2, 3), (LOADW, 0), (EXP, 4), (SEL, 3), (TAKE, 5),
-    (MIXG, 0), (HH, 4), (TAKE, 7), (FIN, 4), (ROWS, 5), (TAKE, 6), (MIXPROD, 0),
-    (ROWS, 7), (EXP, 5), (ROWS, 1), (ROWS, 2), (CONV, 0), (EXP, 7), (SEL, 0),
-    (ROWS, 6), (EXP, 3), (D2, 0), (TAKE, 1), (EXP, 6), (ROWS, 0), (Q2S, 2),
-    (HH, 7), (Q2S, 3), (FIN, 7), (TAKE, 0), (Q2S, 0), (HH, 3), (HH, 6),
-    (TAKE, 2), (EXP, 1), (FIN, 6), (HH, 5), (EXP, 2), (FIN, 3), (Q2S, 1),
-    (EXP, 0), (FIN, 5), (HH, 1), (HH, 2), (CONVG, 0), (FIN, 1), (FIN, 2),
-    (PROJ, 0), (HH, 0), (FIN, 0),
+    (SEL, 7), (MIXP, 0), (SEL, 0), (SEL, 2), (PTAB, 0), (SEL, 3), (M2S, 1),
+    (M2S, 0), (TAKE, 7), (TAKE, 3), (DXW, 0), (D2, 0), (D2, 1), (M2S, 3),
+    (ROWS, 0), (M2S, 2), (SEL, 6), (SEL, 1), (SEL, 5), (ROWS, 7), (SEL, 4),
+    (TAKE, 6), (MIXG, 0), (LOADW, 0), (EXP, 7), (ROWS, 1), (D2, 3), (D2, 2),
+    (TAKE, 4), (TAKE, 1), (COMB, 0), (ROWS, 6), (EXP, 6), (ROWS, 3), (HH, 7),
+    (MIXPROD, 0), (FIN, 7), (EXP, 3), (ROWS, 4), (EXP, 4), (HH, 6), (TAKE, 0),
+    (TAKE, 5), (FIN, 6), (HH, 3), (EXP, 1), (CONV, 0), (HH, 4), (FIN, 4),
+    (EXP, 0), (FIN, 3), (ROWS, 5), (ROWS, 2), (TAKE, 2), (EXP, 5), (EXP, 2),
+    (Q2S, 3), (HH, 0), (Q2S, 1), (HH, 5), (HH, 2), (Q2S, 2), (Q2S, 0),
+    (FIN, 5), (HH, 1), (FIN, 2), (FIN, 1), (CONVG, 0), (FIN, 0), (PROJ, 0),
 )
 
 MIDDLE_STEPS = (
-    (SEL, 4), (SEL, 3), (MIXP, 0), (PTAB, 0), (M2S, 3), (SEL, 1), (SEL, 7),
-    (COMB, 0), (SEL, 5), (DXW, 0), (D2, 3), (M2S, 1), (M2S, 0), (FARW, 4),
-    (GSEL, 4), (GSEL, 5), (TAKE, 4), (TAKE, 1), (TAKE, 7), (D2, 1), (ROWS, 4),
-    (D2, 0), (GSEL, 7), (LOADW, 0), (EXP, 4), (SEL, 6), (SEL, 0), (M2S, 2),
-    (ROWS, 7), (GSEL, 6), (D2, 2), (EXP, 7), (TAKE, 5), (MIXG, 0), (MIXPROD, 0),
-    (TAKE, 3), (HH, 4), (TAKE, 6), (HH, 7), (ROWS, 0), (ROWS, 2), (ROWS, 3),
-    (TAKE, 2), (FIN, 4), (ROWS, 1), (FIN, 7), (EXP, 1), (EXP, 3), (SEL, 2),
-    (ROWS, 6), (CONV, 0), (ROWS, 5), (EXP, 2), (HH, 3), (TAKE, 0), (EXP, 5),
-    (EXP, 0), (EXP, 6), (HH, 1), (Q2S, 2), (HH, 0), (HH, 5), (FIN, 3),
-    (Q2S, 0), (Q2S, 3), (HH, 2), (Q2S, 1), (FIN, 1), (FIN, 5), (FIN, 2),
-    (FIN, 0), (HH, 6), (FIN, 6), (CONVG, 0), (PROJ, 0),
+    (MIXP, 0), (SEL, 0), (M2S, 3), (SEL, 3), (PTAB, 0), (M2S, 1), (M2S, 0),
+    (M2S, 2), (SEL, 1), (DXW, 0), (D2, 3), (FARW, 6), (GSEL, 4), (TAKE, 0),
+    (GSEL, 6), (TAKE, 6), (D2, 0), (GSEL, 7), (D2, 2), (MIXG, 0), (ROWS, 0),
+    (LOADW, 0), (EXP, 0), (ROWS, 6), (EXP, 6), (GSEL, 5), (TAKE, 5), (HH, 6),
+    (SEL, 2), (TAKE, 4), (D2, 1), (FIN, 6), (MIXPROD, 0), (ROWS, 5), (TAKE, 1),
+    (TAKE, 7), (HH, 0), (ROWS, 3), (CONV, 0), (TAKE, 3), (EXP, 3), (ROWS, 4),
+    (ROWS, 2), (TAKE, 2), (EXP, 5), (EXP, 4), (ROWS, 1), (HH, 3), (EXP, 1),
+    (FIN, 3), (HH, 5), (EXP, 2), (FIN, 5), (ROWS, 7), (HH, 4), (Q2S, 0),
+    (HH, 1), (EXP, 7), (Q2S, 1), (FIN, 4), (FIN, 1), (Q2S, 2), (HH, 2),
+    (FIN, 2), (HH, 7), (COMB, 0), (FIN, 7), (Q2S, 3), (CONVG, 0), (PROJ, 0),
+    (FIN, 0),
 )
 
 
@@ -227,8 +227,8 @@
     v_in, v_out, v_val, v_proj, v_gate, v_up, v_down,
     v_mixer, v_expert, v_mixer_gain, v_expert_gain, v_ids, v_shares, taps,
     columns, normed, own_rows, own_table, outgoing, partner_table, combine,
-    rows, arrived, hid, res, returned, gates, ext, rim_out, rim_in, gated, dense, outgoing2, routes, far_rows, far_routes, far_columns, far_tables, far_out,
-    send, recv, send1, recv1, wsem, fsem,
+    rows, arrived, hid, res, returned, gates, ext, rim_out, rim_in, gated, dense, outgoing2, routes, far_rows, far_routes, far_columns, far_tables, far_out, projected, mixed,
+    send, recv, send1, recv1, wsem, fsem, osem,
 ):
     count = outgoing.shape[0]
     group, tok_dev, width = rows.shape
@@ -290,7 +290,6 @@
 
     own_rows[...] = rms_rows(v_expert[...], v_expert_gain[...])
     fill_columns(v_ids, v_shares, routes, columns)
-    own_table[...] = table_of(columns, t)
     pl.semaphore_wait(barrier, count + 1)
 
     def chunk(kind, i, src, dst, dev):
@@ -340,6 +339,7 @@
 
     for_far(lambda copy: copy.start())
     once(DX, own_rows, dense, across).start()
+    own_table[...] = table_of(columns, t)
 
     def farw(i):
         slot = (i - half) // 2 if len(GATES) > 1 else 0
@@ -552,10 +552,11 @@
             total = dot(gated[0], v_proj[0:chan, cols])
             for other in range(1, group):
                 total += dot(gated[other], v_proj[other * chan : (other + 1) * chan, cols])
-            mixer_out[:, cols] = total.astype(BF16)
+            projected[:, cols] = total.astype(BF16)
             return carry
 
         lax.fori_loop(0, chan // tile, one, 0)
+        pltpu.make_async_copy(projected, mixer_out, osem.at[group]).start()
 
     def rest(i):
         pass
@@ -586,7 +587,8 @@
         high = mix.astype(BF16)
         low = (mix - high.astype(F32)).astype(BF16)
         values = returned[:, block].reshape(count * slot_cap, chan)
-        expert_out[part, :] = (dot(high, values) + dot(low, values)).astype(BF16)
+        mixed[part, :] = (dot(high, values) + dot(low, values)).astype(BF16)
+        pltpu.make_async_copy(mixed.at[part], expert_out.at[part], osem.at[block]).start()
 
     def drain(i, carry):
         src = mixed_with(i)
@@ -600,7 +602,7 @@
         def _():
             ret(i).wait_send()
 
-        direct = (i < half) | jnp.where(middle, True, False)
+        direct = (i < half) | jnp.where(middle, False, True)
 
         @pl.when((i != 0) & direct)
         def _():
@@ -618,6 +620,10 @@
 
     lax.fori_loop(0, count, drain, 0)
     for_far(lambda copy: copy.wait_send())
+    pltpu.make_async_copy(projected, mixer_out, osem.at[group]).wait()
+    for block in range(group):
+        part = pl.ds(block * tok_dev, tok_dev)
+        pltpu.make_async_copy(mixed.at[part], expert_out.at[part], osem.at[block]).wait()
 
     @pl.when(middle)
     def _():
@@ -662,7 +668,6 @@
     chan = in_gate_weight.shape[1]
     hid_width = gate_weight.shape[2]
     all_rows = group * tok_dev
-    vm = pl.BlockSpec(memory_space=pltpu.VMEM)
     anywhere = pl.BlockSpec(memory_space=pl.ANY)
     shape = jax.ShapeDtypeStruct
     weights = (
@@ -673,7 +678,7 @@
         exchange_kernel,
         out_shape=(shape((all_rows, chan), BF16), shape((all_rows, chan), BF16)),
         in_specs=[pl.BlockSpec(memory_space=pltpu.HBM)] * 14,
-        out_specs=(vm, vm),
+        out_specs=(pl.BlockSpec(memory_space=pltpu.HBM),) * 2,
         scratch_shapes=[
             pltpu.VMEM(w.shape[-2:], BF16)
             for w in (in_gate_weight, out_gate_weight, value_weight, mixer_proj,
@@ -711,7 +716,9 @@
             pltpu.VMEM((all_rows, 8), F32),
             pltpu.VMEM((len(GATES), experts, slot_cap, tok_dev), BF16),
             pltpu.VMEM((len(GATES), count // 2, slot_cap, width), BF16),
-            dma((14, count)), dma((14, count)), dma((6,)), dma((6,)), dma((7,)), dma((7,)),
+            pltpu.VMEM((all_rows, chan), BF16),
+            pltpu.VMEM((all_rows, chan), BF16),
+            dma((14, count)), dma((14, count)), dma((6,)), dma((6,)), dma((7,)), dma((7,)), dma((group + 1,)),
         ],
         compiler_params=pltpu.CompilerParams(
             collective_id=0, has_side_effects=True, vmem_limit_bytes=VMEM_BYTES

time: 83.6 us -> 77.7 us (0.929)
  Pallas kernels: 82.8 us -> 76.4 us
    pallas_call x1, Pallas kernels: 80.9 us -> 74.5 us  [fused_on_device(): pl.pallas_call(exchange_kernel, out_shape=(shape((all_rows, chan), BF16),...]
where the time goes in v5:
time: 77.7 us; the launch traced here: 77 us
  Pallas kernels  76.4 us (98%)
    pallas_call x1, Pallas kernels, fused_on_device(): pl.pallas_call(exchange_kernel, out_shape=(shape((all_rows, chan), BF16),...  74.5 us
    pallas_call x1, Pallas kernels, fused_on_device(): pl.pallas_call(write_kernel, out_shape=(shape((all_rows, chan), BF16), sh...  1.91 us

profile of v5, /device:TPU:0, one launch (start us, length us, event | category | flops | bytes accessed | tf_op | source)
XLA Modules:
  0.0 77.0 jit_solution(16420025114643132106)
XLA Ops:
  0.6 74.5 %exchange.1 = (bf16[384,512]{1,0:T(8,128)(2,1)}, bf16[384,512]{1,0:T(8,128)(2,1)}) custom-call(bf16[96,2048]{1,0:T(8,128)(2,1)} %mixer_in.1, bf16[96,2048]{1,0:T(8,128)(2,1)} %expert_in.1, f32[1,2048]{1,0:T(1,128)} %bitcast.4, f32[1,2048]{1,0:T(1,128)} %bitcast.5, s32[2,384]{1,0:T(2,128)} %bitcast.6, f32[2,384]{1,0:T(2,128)} %bitcast.7, f32[3,2048]{1,0:T(4,128)} %all_taps.1, ...), custom_call_target="tpu_custom_call" | custom-call | tf_op jit(solution)/shard_map/exchange/pallas_call | solution.py:677
  75.1 1.9 %write.1 = (bf16[384,512]{1,0:T(8,128)(2,1)}, bf16[384,512]{1,0:T(8,128)(2,1)}) custom-call(bf16[384,512]{1,0:T(8,128)(2,1)} %get-tuple-element.4.mixer_sum, bf16[384,512]{1,0:T(8,128)(2,1)} %get-tuple-element.5.expert_sum), custom_call_target="tpu_custom_call" | custom-call | tf_op jit(solution)/shard_map/write/pallas_call | solution.py:731

commit v6 on v5

--- a/solution.py
+++ b/solution.py
@@ -163,6 +163,8 @@
 
 PIECES = 4
 
+CODES = 512
+
 GATES = (6,)
 
 END_STEPS = (
@@ -290,6 +292,7 @@
 
     own_rows[...] = rms_rows(v_expert[...], v_expert_gain[...])
     fill_columns(v_ids, v_shares, routes, columns)
+    own_table[...] = table_of(columns, t)
     pl.semaphore_wait(barrier, count + 1)
 
     def chunk(kind, i, src, dst, dev):
@@ -339,7 +342,6 @@
 
     for_far(lambda copy: copy.start())
     once(DX, own_rows, dense, across).start()
-    own_table[...] = table_of(columns, t)
 
     def farw(i):
         slot = (i - half) // 2 if len(GATES) > 1 else 0
@@ -568,9 +570,15 @@
     steps = max(len(END_STEPS), len(MIDDLE_STEPS))
     tables = [table + ((REST, 0),) * (steps - len(table)) for table in (END_STEPS, MIDDLE_STEPS)]
 
+    packed = [
+        (inner[0] * 16 + inner[1]) * CODES + outer[0] * 16 + outer[1]
+        for outer, inner in zip(*tables)
+    ]
+
     def step(n, carry):
-        at = [[looked_up(list(part), n) for part in zip(*table)] for table in tables]
-        stage, shift = [jnp.where(middle, inner, outer) for outer, inner in zip(*at)]
+        both = looked_up(packed, n)
+        mine = jnp.where(middle, both // CODES, both % CODES)
+        stage, shift = mine // 16, mine % 16
         choose(stage, 0, len(bodies), [functools.partial(body, shift) for body in bodies])
         return carry
 

time: 77.7 us -> 77.1 us (level)
  no operation moved by 1% of the time
where the time goes in v6:
time: 77.1 us; the launch traced here: 76.8 us
  Pallas kernels  76.1 us (99%)
    pallas_call x1, Pallas kernels, fused_on_device(): pl.pallas_call(exchange_kernel, out_shape=(shape((all_rows, chan), BF16),...  74.2 us
    pallas_call x1, Pallas kernels, fused_on_device(): pl.pallas_call(write_kernel, out_shape=(shape((all_rows, chan), BF16), sh...  1.91 us

profile of v6, /device:TPU:0, one launch (start us, length us, event | category | flops | bytes accessed | tf_op | source)
XLA Modules:
  0.0 76.8 jit_solution(6841325005123318691)
XLA Ops:
  0.6 74.2 %exchange.1 = (bf16[384,512]{1,0:T(8,128)(2,1)}, bf16[384,512]{1,0:T(8,128)(2,1)}) custom-call(bf16[96,2048]{1,0:T(8,128)(2,1)} %mixer_in.1, bf16[96,2048]{1,0:T(8,128)(2,1)} %expert_in.1, f32[1,2048]{1,0:T(1,128)} %bitcast.4, f32[1,2048]{1,0:T(1,128)} %bitcast.5, s32[2,384]{1,0:T(2,128)} %bitcast.6, f32[2,384]{1,0:T(2,128)} %bitcast.7, f32[3,2048]{1,0:T(4,128)} %all_taps.1, ...), custom_call_target="tpu_custom_call" | custom-call | tf_op jit(solution)/shard_map/exchange/pallas_call | solution.py:685
  74.9 1.9 %write.1 = (bf16[384,512]{1,0:T(8,128)(2,1)}, bf16[384,512]{1,0:T(8,128)(2,1)}) custom-call(bf16[384,512]{1,0:T(8,128)(2,1)} %get-tuple-element.4.mixer_sum, bf16[384,512]{1,0:T(8,128)(2,1)} %get-tuple-element.5.expert_sum), custom_call_target="tpu_custom_call" | custom-call | tf_op jit(solution)/shard_map/write/pallas_call | solution.py:739

commit v7 on v6

--- a/solution.py
+++ b/solution.py
@@ -284,7 +284,7 @@
     for load in loads:
         load.start()
     picks = v_ids.shape[0]
-    slots = combine.shape[1]
+    slots = combine.shape[2]
 
     def table_of(source, block):
         sent = placed(source, block, tok_dev, picks, slots, slot_cap, False)
@@ -420,7 +420,10 @@
     def comb(i):
         def one(block, carry):
             part = pl.ds(pl.multiple_of(block * tok_dev, tok_dev), tok_dev)
-            combine[part, :] = placed(columns, block, tok_dev, picks, slots, slot_cap, True)
+            mix = placed(columns, block, tok_dev, picks, slots, slot_cap, True)
+            high = mix.astype(BF16)
+            combine[0, part, :] = high
+            combine[1, part, :] = (mix - high.astype(F32)).astype(BF16)
             return carry
 
         lax.fori_loop(0, group, one, 0)
@@ -591,9 +594,7 @@
     lax.fori_loop(1, count, landed, 0)
     for block in range(group):
         part = pl.ds(block * tok_dev, tok_dev)
-        mix = combine[part, :]
-        high = mix.astype(BF16)
-        low = (mix - high.astype(F32)).astype(BF16)
+        high, low = combine[0, part, :], combine[1, part, :]
         values = returned[:, block].reshape(count * slot_cap, chan)
         mixed[part, :] = (dot(high, values) + dot(low, values)).astype(BF16)
         pltpu.make_async_copy(mixed.at[part], expert_out.at[part], osem.at[block]).start()
@@ -705,7 +706,7 @@
             pltpu.VMEM((experts, slot_cap, tok_dev), BF16),
             pltpu.VMEM((experts, slot_cap, width), BF16),
             pltpu.VMEM((experts, slot_cap, tok_dev), BF16),
-            pltpu.VMEM((all_rows, experts * slot_cap), F32),
+            pltpu.VMEM((2, all_rows, experts * slot_cap), BF16),
             pltpu.VMEM((group, tok_dev, width), BF16),
             pltpu.VMEM((count, group, slot_cap, width), BF16),
             pltpu.VMEM((count, group, group * slot_cap, hid_width), BF16),

time: 77.1 us -> 77.1 us (level)
  no operation moved by 1% of the time
where the time goes in v7:
time: 77.1 us; the launch traced here: 76.8 us
  Pallas kernels  76.1 us (99%)
    pallas_call x1, Pallas kernels, fused_on_device(): pl.pallas_call(exchange_kernel, out_shape=(shape((all_rows, chan), BF16),...  74.2 us
    pallas_call x1, Pallas kernels, fused_on_device(): pl.pallas_call(write_kernel, out_shape=(shape((all_rows, chan), BF16), sh...  1.91 us

profile of v7, /device:TPU:0, one launch (start us, length us, event | category | flops | bytes accessed | tf_op | source)
XLA Modules:
  0.0 76.8 jit_solution(10274689855647098699)
XLA Ops:
  0.6 74.2 %exchange.1 = (bf16[384,512]{1,0:T(8,128)(2,1)}, bf16[384,512]{1,0:T(8,128)(2,1)}) custom-call(bf16[96,2048]{1,0:T(8,128)(2,1)} %mixer_in.1, bf16[96,2048]{1,0:T(8,128)(2,1)} %expert_in.1, f32[1,2048]{1,0:T(1,128)} %bitcast.4, f32[1,2048]{1,0:T(1,128)} %bitcast.5, s32[2,384]{1,0:T(2,128)} %bitcast.6, f32[2,384]{1,0:T(2,128)} %bitcast.7, f32[3,2048]{1,0:T(4,128)} %all_taps.1, ...), custom_call_target="tpu_custom_call" | custom-call | tf_op jit(solution)/shard_map/exchange/pallas_call | solution.py:686
  74.9 1.9 %write.1 = (bf16[384,512]{1,0:T(8,128)(2,1)}, bf16[384,512]{1,0:T(8,128)(2,1)}) custom-call(bf16[384,512]{1,0:T(8,128)(2,1)} %get-tuple-element.4.mixer_sum, bf16[384,512]{1,0:T(8,128)(2,1)} %get-tuple-element.5.expert_sum), custom_call_target="tpu_custom_call" | custom-call | tf_op jit(solution)/shard_map/write/pallas_call | solution.py:740
